TPU v7x, 512 devices: a whole 4x8x8 slice. The times are simulated.
512 devices in a mesh: sp: 64 (over z, y), tp: 8 (over x, core).
Axes of the slice: x: 4, y: 8, z: 8, core: 2. Of those that a mesh axis runs over, the one named last changes fastest.
Arguments:
- latent_tokens: bfloat16 [8192, 2048], P(('sp', 'tp')), may hold values from -6 to 6
- context_tokens: bfloat16 [512, 2048], P('sp'), may hold values from -6 to 6
- cond: float32 [2048], replicated, may hold values from -6 to 6
- ctx_cond: float32 [2048], replicated, may hold values from -6 to 6
- mod_shift: bfloat16 [2048, 2048], P('sp', 'tp'), may hold values from -0.125 to 0.125
- mod_scale: bfloat16 [2048, 2048], P('sp', 'tp'), may hold values from -0.125 to 0.125
- mod_gate: bfloat16 [2048, 2048], P('sp', 'tp'), may hold values from -0.125 to 0.125
- norm_gain: float32 [2048], replicated, may hold values from 0.1 to 1.9
- w_query: bfloat16 [2048, 1536], P(None, 'tp'), may hold values from -0.125 to 0.125
- query_gain: float32 [96], replicated, may hold values from 0.8 to 2
- w_down_kv: bfloat16 [2048, 256], replicated, may hold values from -0.125 to 0.125
- w_rope_key: bfloat16 [2048, 32], replicated, may hold values from -0.125 to 0.125
- kv_gain: float32 [256], replicated, may hold values from 0.1 to 1.9
- w_up_kv: bfloat16 [2, 256, 1024], P(None, None, 'tp'), may hold values from -0.375 to 0.375
- key_gain: float32 [96], replicated, may hold values from 0.8 to 2
- ctx_lift: float32 [16], P('tp'), may hold values from 1.5 to 220
- w_output: bfloat16 [1024, 2048], P('tp'), may hold values from -0.1875 to 0.1875
Outputs:
- updated: bfloat16 [8192, 2048], P(('sp', 'tp'))
All inputs are finite; a program needn't handle non-finite values.
Results may differ from a plain program's by a relative error of at most 0.007.
Values may be sent and summed in bfloat16 or wider, within the bound.
A program may use at most 64 MiB of HBM per device.

v0:
```python
import functools

import jax
import jax.numpy as jnp
from jax import lax
from jax.sharding import Mesh
from jax.sharding import PartitionSpec as P

HD = 64
ROPE = 32
QK = 96
GRID_W = 64
SP = ("sp_0", "sp_1")
SP_TP = ("sp_0", "sp_1", "tp")


EPS = 1e-06
THETA = 10000.0


def over_axes(value, axes):
    return functools.reduce(lax.psum, axes, value)


def in_one_piece(arrays, axis, dim, along):
    ends, at = ([], 0)
    for a in arrays[:-1]:
        at += a.shape[along]
        ends.append(at)
    both = jnp.concatenate(arrays, axis=along)
    return tuple(jnp.split(lax.all_gather(both, axis, axis=dim, tiled=True), ends, axis=along))


def copy_for_each(value, axis):
    copies = jnp.broadcast_to(value, (lax.axis_size(axis), *value.shape))
    return lax.all_to_all(copies, axis, split_axis=0, concat_axis=0, tiled=True)


def joined_along(tiles, dim):
    tiles = jnp.moveaxis(tiles, 0, dim)
    shape = tiles.shape
    return tiles.reshape(*shape[:dim], shape[dim] * shape[dim + 1], *shape[dim + 2 :])


def collect(value, axis, dim):
    tiles = copy_for_each(value, axis)
    return joined_along(tiles, dim)


def split_up(value, dim, count):
    shape = value.shape
    tiles = value.reshape(*shape[:dim], count, shape[dim] // count, *shape[dim + 1 :])
    return jnp.moveaxis(tiles, dim, 0)


def sent_and_summed(value, axis, dim):
    count = lax.axis_size(axis)
    tiles = lax.all_to_all(split_up(value, dim, count), axis, 0, 0, tiled=True)
    return jnp.sum(tiles.astype(jnp.float32), axis=0)


def rms_normed(values, gain_vector):
    values = values.astype(jnp.float32)
    inv_root = lax.rsqrt(jnp.mean(values * values, axis=-1, keepdims=True) + EPS)
    return values * inv_root * gain_vector


def grid_angles(position, width):
    freq_count = width // 4
    inverse = THETA ** (-jnp.arange(freq_count, dtype=jnp.float32) / freq_count)
    row_index = (position // GRID_W).astype(jnp.float32)
    col_index = (position % GRID_W).astype(jnp.float32)
    return jnp.concatenate([row_index[:, None] * inverse, col_index[:, None] * inverse], axis=-1)


def rotate_tail(head_rows, angle, plain):
    tail = head_rows[..., plain:]
    half_width = tail.shape[-1] // 2
    cosine = jnp.cos(angle)[:, None, :]
    sine_val = jnp.sin(angle)[:, None, :]
    front_half = tail[..., :half_width]
    back_half = tail[..., half_width:]
    return jnp.concatenate(
        [
            head_rows[..., :plain],
            front_half * cosine - back_half * sine_val,
            back_half * cosine + front_half * sine_val,
        ],
        axis=-1,
    )


def modulation(signal, weight):
    return jnp.dot(signal, weight.astype(jnp.float32))


def compress(hidden, w_down_kv, w_rope_key, kv_gain):
    latent = rms_normed(jnp.dot(hidden, w_down_kv, preferred_element_type=jnp.float32), kv_gain)
    rope_key = jnp.dot(hidden, w_rope_key, preferred_element_type=jnp.float32)
    return (latent.astype(jnp.bfloat16), rope_key.astype(jnp.bfloat16))


def expand(latent, rope_key, w_up_kv, key_gain, angle):
    row_count = latent.shape[0]
    head_count = w_up_kv.shape[2] // HD
    key_plain = jnp.dot(latent, w_up_kv[0], preferred_element_type=jnp.float32).reshape(
        row_count, head_count, HD
    )
    shared = jnp.broadcast_to(
        rope_key.astype(jnp.float32)[:, None, :], (row_count, head_count, ROPE)
    )
    keys = rms_normed(jnp.concatenate([key_plain, shared], axis=-1), key_gain)
    if angle is not None:
        keys = rotate_tail(keys, angle, HD)
    values = jnp.dot(latent, w_up_kv[1], preferred_element_type=jnp.float32).astype(jnp.bfloat16)
    return (keys.astype(jnp.bfloat16), values.reshape(row_count, head_count, HD))


def absorb(carry, query_heads, keys, values, lift):
    highest, total, mixed = carry
    scores = (
        jnp.einsum("qhd,khd->hqk", query_heads, keys, preferred_element_type=jnp.float32)
        * QK ** (-0.5)
        + lift
    )
    new_high = jnp.maximum(highest, jnp.max(scores, axis=-1))
    weights = jnp.exp(scores - new_high[:, :, None])
    factor = jnp.exp(highest - new_high)
    total = total * factor + jnp.sum(weights, axis=-1)
    update = jnp.einsum(
        "hqk,khd->qhd", weights.astype(jnp.bfloat16), values, preferred_element_type=jnp.float32
    )
    mixed = mixed * jnp.transpose(factor)[:, :, None] + update
    return (new_high, total, mixed)


def local(
    latent_tokens,
    context_tokens,
    cond,
    ctx_cond,
    mod_shift,
    mod_scale,
    mod_gate,
    norm_gain,
    w_query,
    query_gain,
    w_down_kv,
    w_rope_key,
    kv_gain,
    w_up_kv,
    key_gain,
    ctx_lift,
    w_output,
):
    tp_count = lax.axis_size("tp")
    sp_index = lax.axis_index(SP)
    piece_rows = mod_shift.shape[0]
    own_start = sp_index * piece_rows
    lat_signal = jax.nn.silu(lax.dynamic_slice_in_dim(cond, own_start, piece_rows, 0))
    ctx_signal = jax.nn.silu(lax.dynamic_slice_in_dim(ctx_cond, own_start, piece_rows, 0))
    both_signal = jnp.stack([lat_signal, ctx_signal])
    shift_part = modulation(both_signal, mod_shift)
    scale_part = modulation(both_signal, mod_scale)
    gate_part = modulation(lat_signal[None, :], mod_gate)
    shift_sum, scale_sum, gate_sum = (
        over_axes(shift_part, SP),
        over_axes(scale_part, SP),
        over_axes(gate_part, SP),
    )
    shift_vec, scale_vec, gate_vec = in_one_piece((shift_sum, scale_sum, gate_sum), "tp", 1, 0)
    hidden_lat = (
        rms_normed(latent_tokens, norm_gain) * (1.0 + scale_vec[0]) + shift_vec[0]
    ).astype(jnp.bfloat16)
    ctx_rows = lax.all_gather(context_tokens, SP, axis=0, tiled=True)
    ctx_hidden = (rms_normed(ctx_rows, norm_gain) * (1.0 + scale_vec[1]) + shift_vec[1]).astype(
        jnp.bfloat16
    )
    ctx_latent, ctx_rope = compress(ctx_hidden, w_down_kv, w_rope_key, kv_gain)
    ctx_keys, ctx_values = expand(ctx_latent, ctx_rope, w_up_kv, key_gain, None)
    head_count = ctx_lift.shape[0]
    local_rows = latent_tokens.shape[0]
    group_rows = local_rows * tp_count
    group_start = sp_index * group_rows
    qk_width = head_count * QK
    piece = collect(hidden_lat, "tp", 0)
    row_count = piece.shape[0]
    position = group_start + jnp.arange(row_count, dtype=jnp.int32)
    latent, rope_key = compress(piece, w_down_kv, w_rope_key, kv_gain)
    keys, values = expand(latent, rope_key, w_up_kv, key_gain, grid_angles(position, ROPE))
    make_row_count = piece.shape[0]
    position = group_start + jnp.arange(make_row_count, dtype=jnp.int32)
    raw = jnp.dot(piece, w_query, preferred_element_type=jnp.float32).reshape(
        make_row_count, head_count, QK
    )
    turned = rotate_tail(rms_normed(raw, query_gain), grid_angles(position, ROPE), HD)
    projected = jnp.concatenate(
        [
            turned.astype(jnp.bfloat16).reshape(make_row_count, qk_width),
            keys.reshape(row_count, qk_width),
            values.reshape(row_count, head_count * HD),
        ],
        axis=1,
    )
    queries = projected[:, :qk_width]
    group_keys = projected[:, qk_width : 2 * qk_width]
    group_values = projected[:, 2 * qk_width :]
    query_heads = queries.reshape(group_rows, head_count, QK)
    start_carry = (
        jnp.full((head_count, group_rows), -1e30, jnp.float32),
        jnp.zeros((head_count, group_rows), jnp.float32),
        jnp.zeros((group_rows, head_count, HD), jnp.float32),
    )
    carry = absorb(start_carry, query_heads, ctx_keys, ctx_values, ctx_lift[:, None, None])
    pieces = in_one_piece((group_keys, group_values), SP, 0, 1)
    row_count = pieces[0].shape[0]
    keys = pieces[0].reshape(row_count, head_count, QK)
    values = pieces[1].reshape(row_count, head_count, HD)
    carry = absorb(carry, query_heads, keys, values, 0.0)
    highest, total, mixed = carry
    attended = (
        (mixed / jnp.transpose(total)[:, :, None])
        .astype(jnp.bfloat16)
        .reshape(group_rows, head_count * HD)
    )
    out = sent_and_summed(
        jnp.dot(attended, w_output, preferred_element_type=jnp.float32).astype(jnp.bfloat16),
        "tp",
        0,
    )
    return (latent_tokens.astype(jnp.float32) + gate_vec[0] * out).astype(jnp.bfloat16)


def solution(mesh):
    finer = Mesh(mesh.devices.reshape(8, 8, mesh.shape["tp"]), ("sp_0", "sp_1", "tp"))
    in_specs = (
        P(SP_TP, None),
        P(SP, None),
        P(),
        P(),
        P(SP, "tp"),
        P(SP, "tp"),
        P(SP, "tp"),
        P(),
        P(None, "tp"),
        P(),
        P(),
        P(),
        P(),
        P(None, None, "tp"),
        P(),
        P("tp"),
        P("tp", None),
    )
    out_specs = P(SP_TP, None)
    return jax.shard_map(local, mesh=finer, in_specs=in_specs, out_specs=out_specs, check_vma=False)
```

profile of v0, /device:TPU:1, one launch (start us, length us, event | category | flops | bytes accessed | tf_op | source)
XLA Modules:
  0.0 226.2 jit_solution(14526996260051699909)
XLA Ops:
  6.5 0.0 copy-start
  6.5 0.0 copy-start.2
  6.6 0.0 copy-start.9
  6.6 0.0 all-gather.3.cloned.1.call-start
  6.6 0.7 all-gather.3.cloned.1.call-update
  7.3 0.9 fusion.51
  8.2 0.8 fusion.53
  9.0 0.8 fusion.55
  9.9 0.8 fusion.56
  10.7 20.5 %all-reduce.1 = (f32[1,256]{1,0:T(1,128)S(1)}, f32[2,256]{1,0:T(2,128)S(1)}, f32[2,256]{1,0:T(2,128)S(1)}) all-reduce(f32[1,256]{1,0:T(1,128)S(1)} %fusion.51, f32[2,256]{1,0:T(2,128)S(1)} %fusion.55, f32[2,256]{1,0:T(2,128)S(1)} %fusion.56), channel_id=1, replica_groups=mesh['sp_0'=8,'sp_1'=8,'tp'=8] {'sp_0'}, use_global_device_ids=true, to_apply=%region_4.5 | all-reduce | flops 1280 | bytes 10240 | tf_op jit(solution)/shard_map/psum | solution.py:22
  31.2 14.8 %all-reduce = (f32[1,256]{1,0:T(1,128)S(1)}, f32[2,256]{1,0:T(2,128)S(1)}, f32[2,256]{1,0:T(2,128)S(1)}) all-reduce(f32[1,256]{1,0:T(1,128)S(1)} %get-tuple-element.8, f32[2,256]{1,0:T(2,128)S(1)} %get-tuple-element.9, f32[2,256]{1,0:T(2,128)S(1)} %get-tuple-element.10), channel_id=1, replica_groups=mesh['sp_0'=8,'sp_1'=8,'tp'=8] {'sp_1'}, use_global_device_ids=true, to_apply=%region_5.6 | all-reduce | flops 1280 | bytes 10240 | tf_op jit(solution)/shard_map/psum | solution.py:22
  46.0 20.5 %all_gather.9 = f32[5,2048]{1,0:T(8,128)S(1)} all-gather(f32[5,256]{1,0:T(8,128)S(1)} %pad_maximum_fusion.7), channel_id=1, replica_groups=mesh['sp_0'=8,'sp_1'=8,'tp'=8] {'tp'}, dimensions={1}, use_global_device_ids=true | all-gather | bytes 46080 | tf_op jit(solution)/shard_map/all_gather | solution.py:31
  66.5 1.0 fusion.29
  67.4 0.9 fusion.33
  68.4 0.8 broadcast_in_dim.13
  69.2 3.9 %all-to-all-start = ((bf16[8,16,2048]{2,1,0:T(8,128)(2,1)}), bf16[8,16,2048]{2,1,0:T(8,128)(2,1)S(1)}, u32[]{:S(2)}, u32[]{:S(2)}) async-start(bf16[8,16,2048]{2,1,0:T(8,128)(2,1)} %broadcast_in_dim.13), calls=%async_computation | async-start | bytes 1048576 | tf_op jit(solution)/shard_map/all_to_all | solution.py:36
  73.1 0.0 all-gather.5.cloned.1.call-start
  73.1 0.9 slice_bitcast_fusion
  74.0 0.1 copy.18
  74.1 0.1 broadcast_multiply_fusion.1
  74.2 0.1 fusion.45
  74.2 8.2 %all-to-all-done = bf16[8,16,2048]{2,1,0:T(8,128)(2,1)S(1)} async-done(((bf16[8,16,2048]{2,1,0:T(8,128)(2,1)}), bf16[8,16,2048]{2,1,0:T(8,128)(2,1)S(1)}, u32[]{:S(2)}, u32[]{:S(2)}) %all-to-all-start) | async-done | bytes 524320 | tf_op jit(solution)/shard_map/all_to_all | solution.py:36
  82.4 0.0 copy-done
  82.4 0.4 multiply_reduce_fusion.2
  82.8 0.0 copy-done.7
  82.9 0.2 fusion.38
  83.1 0.0 copy-done.6
  83.1 0.3 fusion.20
  83.4 0.0 copy-done.10
  83.5 0.1 multiply_multiply_fusion
  83.6 0.0 copy-done.2
  83.6 0.4 multiply_reduce_fusion.4
  84.0 0.0 copy-done.9
  84.0 0.1 multiply_multiply_fusion.1
  84.1 0.0 copy-done.5
  84.1 0.3 convolution_convert_fusion.2
  84.3 0.6 pad_maximum_fusion.2
  85.0 0.0 all-gather.5.cloned.1.call-update
  85.0 10.3 %all-gather.3.cloned.1.call-done = bf16[512,2048]{1,0:T(8,128)(2,1)} async-done(((bf16[8,2048]{1,0:T(8,128)(2,1)}), bf16[512,2048]{1,0:T(8,128)(2,1)}) %all-gather.3.cloned.1.call-update) | async-done | bytes 2097168 | tf_op jit(solution)/shard_map/all_gather | solution.py:175
  95.3 2.1 fusion.2
  97.4 0.0 copy-done.8
  97.4 0.0 copy-start.1
  97.4 2.9 %multiply_reduce_fusion = (f32[512]{0:T(512)S(1)}, f32[512,256]{0,1:T(8,128)S(1)}) fusion(bf16[2048,256]{1,0:T(8,128)(2,1)S(1)} %copy-done, bf16[512,2048]{1,0:T(8,128)(2,1)} %all-gather.3.cloned.1.call-done, f32[2048]{0:T(1024)S(1)} %bitcast.109, f32[2048]{0:T(1024)S(1)} %bitcast.111, f32[2048]{0:T(1024)S(1)} %copy-done.8, f32[512]{0:T(512)S(1)} %add_rsqrt_fusion.2), kind=kOutput, calls=%fused_computation.32 | convolution fusion | flops 543424000 | bytes 3698688 | tf_op jit(solution)/shard_map/dot_general | solution.py:98
  100.3 0.0 copy-start.11
  100.3 0.3 fusion.24
  100.6 0.0 copy-done.1
  100.6 1.0 fusion.19
  101.6 0.1 multiply_reduce_fusion.1
  101.7 0.0 copy-done.11
  101.7 0.4 fusion.66
  102.1 0.3 convolution_convert_fusion.1
  102.4 88.4 %all-gather.5.cloned.1.call-done = bf16[8192,320]{0,1:T(8,128)(2,1)} async-done(((bf16[128,320]{0,1:T(8,128)(2,1)}), bf16[8192,320]{0,1:T(8,128)(2,1)}) %all-gather.5.cloned.1.call-update) | async-done | bytes 5242896 | tf_op jit(solution)/shard_map/all_gather | solution.py:31
  190.8 1.9 slice-done
  192.7 1.4 fusion.67
  194.1 1.4 fusion
  195.5 1.6 slice-done.1
  197.1 1.7 fusion.11
  198.8 0.2 fusion.21
  199.0 0.3 fusion.18
  199.3 0.0 copy-done.4
  199.4 0.3 convolution_convert_fusion
  199.7 18.9 %all_to_all.10 = bf16[8,16,2048]{2,1,0:T(8,128)(2,1)S(1)} all-to-all(bf16[8,16,2048]{2,1,0:T(8,128)(2,1)S(1)} %bitcast.99), channel_id=1, replica_groups=mesh['sp_0'=8,'sp_1'=8,'tp'=8] {'tp'}, dimensions={0} | all-to-all | bytes 1048576 | tf_op jit(solution)/shard_map/all_to_all | solution.py:58
  218.6 0.1 convert_reduce_fusion
  218.7 0.7 fusion.34
  (30 shorter events, 0.3 us)
Async XLA Ops:
  6.5 75.9 %copy-start = (bf16[2048,256]{1,0:T(8,128)(2,1)S(1)}, bf16[2048,256]{1,0:T(8,128)(2,1)}, u32[]{:S(2)}) copy-start(bf16[2048,256]{1,0:T(8,128)(2,1)} %param.27) | copy-start | bytes 3145732
  6.5 77.5 %copy-start.5 = (bf16[2,256,128]{2,1,0:T(8,128)(2,1)S(1)}, bf16[2,256,128]{2,1,0:T(8,128)(2,1)}, u32[]{:S(2)}) copy-start(bf16[2,256,128]{2,1,0:T(8,128)(2,1)} %param.30) | copy-start | bytes 393220
  6.5 76.3 %copy-start.7 = (f32[256]{0:T(256)S(1)}, f32[256]{0:T(256)}, u32[]{:S(2)}) copy-start(f32[256]{0:T(256)} %param.29) | copy-start | bytes 3076
  6.5 76.5 %copy-start.6 = (bf16[2048,32]{0,1:T(8,128)(2,1)S(1)}, bf16[2048,32]{0,1:T(8,128)(2,1)}, u32[]{:S(2)}) copy-start(bf16[2048,32]{0,1:T(8,128)(2,1)} %param.28) | copy-start | bytes 393220
  6.5 76.9 %copy-start.10 = (f32[96]{0:T(128)S(1)}, f32[96]{0:T(128)}, u32[]{:S(2)}) copy-start(f32[96]{0:T(128)} %param.31) | copy-start | bytes 1156
  6.5 77.0 %copy-start.2 = (bf16[2048,192]{0,1:T(8,128)(2,1)S(1)}, bf16[2048,192]{0,1:T(8,128)(2,1)}, u32[]{:S(2)}) copy-start(bf16[2048,192]{0,1:T(8,128)(2,1)} %param.25) | copy-start | bytes 2359300
  6.6 77.4 %copy-start.9 = (f32[96]{0:T(128)S(1)}, f32[96]{0:T(128)}, u32[]{:S(2)}) copy-start(f32[96]{0:T(128)} %param.26) | copy-start | bytes 1156
  6.6 88.7 %all-gather.3.cloned.1.call-start = ((), (), s32[]{:S(2)}) async-start(), calls=%async_computation.2 | async-start | bytes 2129920 | tf_op jit(solution)/shard_map/all_gather | solution.py:175
  69.2 13.2 %all-to-all-start = ((bf16[8,16,2048]{2,1,0:T(8,128)(2,1)}), bf16[8,16,2048]{2,1,0:T(8,128)(2,1)S(1)}, u32[]{:S(2)}, u32[]{:S(2)}) async-start(bf16[8,16,2048]{2,1,0:T(8,128)(2,1)} %broadcast_in_dim.13), calls=%async_computation | async-start | bytes 1048576 | tf_op jit(solution)/shard_map/all_to_all | solution.py:36
  73.1 24.3 %copy-start.8 = (f32[2048]{0:T(1024)S(1)}, f32[2048]{0:T(1024)}, u32[]{:S(2)}) copy-start(f32[2048]{0:T(1024)} %param.24) | copy-start | bytes 24580
  73.1 117.7 %all-gather.5.cloned.1.call-start = ((), (), s32[]{:S(2)}) async-start(), calls=%async_computation.3 | async-start | bytes 5324800 | tf_op jit(solution)/shard_map/all_gather | solution.py:31
  97.4 3.2 %copy-start.1 = (bf16[512,2048]{1,0:T(8,128)(2,1)S(1)}, bf16[512,2048]{1,0:T(8,128)(2,1)}, u32[]{:S(2)}) copy-start(bf16[512,2048]{1,0:T(8,128)(2,1)} %all-gather.3.cloned.1.call-done) | copy-start | bytes 6291460
  100.3 1.4 copy-start.11
  190.8 1.9 slice-start
  195.5 1.6 slice-start.1
  197.1 2.3 %copy-start.4 = (bf16[128,2048]{1,0:T(8,128)(2,1)S(1)}, bf16[128,2048]{1,0:T(8,128)(2,1)}, u32[]{:S(2)}) copy-start(bf16[128,2048]{1,0:T(8,128)(2,1)} %param.33) | copy-start | bytes 1572868
  197.1 21.6 %copy-start.3 = (bf16[16,2048]{1,0:T(8,128)(2,1)S(1)}, bf16[16,2048]{1,0:T(8,128)(2,1)}, u32[]{:S(2)}) copy-start(bf16[16,2048]{1,0:T(8,128)(2,1)} %param.17) | copy-start | bytes 196612
Sparse Core Ops, SparseCore 0:
  10.4 84.8 all-gather.2
  98.3 92.4 all-gather.4
where the time goes:
time: 227 us; the launch traced here: 226 us
  waiting for transfers between devices  108 us (48%)
  blocking collectives  74.6 us (33%)
  between operations  13.7 us (6%)
  matrix products  12.7 us (6%)
  other arithmetic  8.28 us (4%)
  local copies, waits for them, and re-layouts  5.41 us (2%)
  starting transfers between devices  3.9 us (2%)
    all_gather x1, waiting for transfers between devices, in_one_piece(): lax.all_gather(both, axis, axis=dim, tiled=True)  88.4 us
    psum x2, blocking collectives, over_axes(): return functools.reduce(lax.psum, axes, value)  35.2 us
    all_gather x1, blocking collectives, in_one_piece(): lax.all_gather(both, axis, axis=dim, tiled=True)  20.5 us
    all_to_all x1, blocking collectives, sent_and_summed(): tiles = lax.all_to_all(split_up(value, dim, count), axis, 0, 0, tiled=True)  18.9 us
    all_gather x1, waiting for transfers between devices, local(): ctx_rows = lax.all_gather(context_tokens, SP, axis=0, tiled=True)  10.3 us
    all_to_all x1, waiting for transfers between devices, copy_for_each(): return lax.all_to_all(copies, axis, split_axis=0, concat_axis=0, tiled=True)  8.21 us
  transfers between devices with their start and end apart: 3, of which 3 were waited for; matrix products, arithmetic and copies ran while one was open for 7% of the time, Pallas kernels for 0%

commit v1 on v0

v1 whole, which is shorter than its diff:
```python
import functools
import math

import jax
import jax.numpy as jnp
from jax import lax
from jax.experimental import pallas as pl
from jax.experimental.pallas import tpu as pltpu
from jax.sharding import PartitionSpec as P

HD = 64
ROPE = 32
QK = 96
KVL = 256
HALF = ROPE // 2
GRID_W = 64
EPS = 1e-06
THETA = 10000.0
LOG2E = math.log2(math.e)
MESH = pl.DeviceIdType.MESH
F32 = jnp.float32
BF16 = jnp.bfloat16
HIGHEST = lax.Precision.HIGHEST
LANES = 128
MSG = 80


def nt_dot(a, b):
    return lax.dot_general(a, b, (((1,), (1,)), ((), ())), preferred_element_type=F32)


def lane_ids(shape):
    return lax.broadcasted_iota(jnp.int32, shape, 1)


def row_ids(shape):
    return lax.broadcasted_iota(jnp.int32, shape, 0)


def silu(v):
    return v / (1.0 + jnp.exp(-v))


def column_tile(row):
    width = row.shape[1]
    full = jnp.concatenate([row, jnp.zeros((1, LANES - width), F32)], axis=1)
    return jnp.broadcast_to(full, (LANES, LANES)).T


def angle_tables(group):
    shape = (HALF, LANES)
    freq_row = row_ids(shape)
    token = lane_ids(shape)
    inverse = jnp.zeros(shape, F32)
    for j in range(HALF // 2):
        inverse = jnp.where(freq_row % (HALF // 2) == j, THETA ** (-j / (HALF // 2)), inverse)
    row = (group * (LANES // GRID_W) + token // GRID_W).astype(F32)
    col = (token % GRID_W).astype(F32)
    angle = jnp.where(freq_row < HALF // 2, row, col) * inverse
    return jnp.cos(angle), jnp.sin(angle)


def rotated(tail, cosine, sine):
    front, back = tail[:HALF], tail[HALF:]
    return jnp.concatenate([front * cosine - back * sine, back * cosine + front * sine], axis=0)


def kernel(
    nz,
    ny,
    ntp,
    tok_h,
    ctx_h,
    cond_h,
    cctx_h,
    mshift_h,
    mscale_h,
    mgate_h,
    ngain_h,
    wq_h,
    qgain_h,
    wdown_h,
    wrope_h,
    kvgain_h,
    wup_h,
    kgain_h,
    lift_s,
    wout_h,
    out_ref,
    gtok,
    ctok,
    cond_v,
    cctx_v,
    mods,
    ngain,
    wq,
    qgain,
    wdown,
    wrope,
    kvgain,
    wup,
    kgain,
    wout,
    zbuf,
    ybuf,
    tbuf,
    nv,
    nvc,
    hid,
    wupt,
    ctab,
    stab,
    msg,
    qbuf,
    qfull,
    keys,
    vals,
    ctxl,
    ctxr,
    ostage,
    obuf,
    rstage,
    rbuf,
    load_sem,
    send_sem,
    recv_sem,
    fwd_send,
    fwd_recv,
):
    sp = lax.axis_index("sp")
    tp = lax.axis_index("tp")
    zi, yi = sp // ny, sp % ny
    core = tp % 2
    rows = tok_h.shape[0]
    width = tok_h.shape[1]
    piece = mods.shape[2]
    crow = ctx_h.shape[0]
    nlat = nz * LANES

    def z_peer(k):
        return (((zi + k) % nz) * ny + yi, tp)

    def y_peer(k):
        return (zi * ny + (yi + k) % ny, tp)

    def t_peer(k):
        return (sp, (tp + k) % ntp)

    sibling = (sp, tp + 1 - 2 * core)

    pairs = [
        (cond_h, cond_v),
        (cctx_h, cctx_v),
        (mshift_h, mods.at[0]),
        (mscale_h, mods.at[1]),
        (mgate_h, mods.at[2]),
        (tok_h, gtok.at[tp]),
        (ctx_h, ctok),
        (ngain_h, ngain),
        (wup_h, wup),
        (kgain_h, kgain),
        (qgain_h, qgain),
        (kvgain_h, kvgain),
        (wdown_h, wdown),
        (wrope_h, wrope),
        (wq_h, wq),
        (wout_h, wout),
    ]
    loads = [pltpu.make_async_copy(a, b, load_sem.at[i]) for i, (a, b) in enumerate(pairs)]
    for copy in loads:
        copy.start()

    barrier = pltpu.get_barrier_semaphore()
    peers = (
        [z_peer(k) for k in range(1, nz)]
        + [y_peer(k) for k in range(1, ny)]
        + [t_peer(k) for k in range(1, ntp)]
    )
    for peer in peers:
        pl.semaphore_signal(barrier, inc=1, device_id=peer, device_id_type=MESH)

    for i in range(5):
        loads[i].wait()
    mod_rows = mods.shape[1]
    fold = LANES // mod_rows
    quarter = sp % fold
    own_row = sp // fold
    lat_row = silu(cond_v[pl.ds(own_row, 1), :])
    ctx_row = silu(cctx_v[pl.ds(own_row, 1), :])
    mine = lane_ids((1, LANES)) // mod_rows == quarter
    signal = jnp.concatenate(
        [jnp.where(mine, lat_row, 0.0), jnp.where(mine, ctx_row, 0.0), jnp.zeros((6, LANES), F32)],
        axis=0,
    )
    block = jnp.concatenate([mods[0], mods[1], mods[2]], axis=1).astype(F32)
    block = jnp.concatenate([block] * fold, axis=0)
    share = jnp.dot(signal, block, precision=HIGHEST, preferred_element_type=F32)
    zbuf[0] = share[0:2]

    pl.semaphore_wait(barrier, len(peers))

    def exchange(src, buf, count, peer, first):
        copies = []
        for k in range(1, count):
            copies.append(
                pltpu.make_async_remote_copy(
                    src_ref=src,
                    dst_ref=buf.at[k],
                    send_sem=send_sem.at[first + k],
                    recv_sem=recv_sem.at[first + k],
                    device_id=peer(k),
                    device_id_type=MESH,
                )
            )
        for copy in copies:
            copy.start()
        return copies

    z_copies = exchange(zbuf.at[0], zbuf, nz, z_peer, 0)

    loads[5].wait()
    tok_copies = []
    for k in range(1, ntp):
        tok_copies.append(
            pltpu.make_async_remote_copy(
                src_ref=gtok.at[tp],
                dst_ref=gtok.at[tp],
                send_sem=send_sem.at[8 + k],
                recv_sem=recv_sem.at[8 + k],
                device_id=t_peer(k),
                device_id_type=MESH,
            )
        )
    for copy in tok_copies:
        copy.start()

    for i in range(6, 12):
        loads[i].wait()
    gain_row = ngain[...]
    cv = ctok[...].astype(F32)
    nvc[...] = cv * lax.rsqrt(jnp.mean(cv * cv, axis=1, keepdims=True) + EPS) * gain_row
    wupt[...] = wup[0].astype(F32).T.astype(BF16)
    keys[...] = jnp.zeros(keys.shape, BF16)
    vals[:, nlat:, :] = jnp.zeros((2, LANES, LANES), BF16)
    ctxl[...] = jnp.zeros(ctxl.shape, F32)
    ctxr[...] = jnp.zeros(ctxr.shape, F32)
    msg[0, :, 64:80, :] = jnp.zeros((2, 16, KVL), BF16)
    hid[LANES:, :] = jnp.zeros((hid.shape[0] - LANES, width), BF16)
    kg = column_tile(kgain[...])
    qg = column_tile(qgain[...]) * (LOG2E * QK ** (-0.5))
    for k in range(nz):
        cosine, sine = angle_tables(((zi + nz - k) % nz) * ny + yi)
        ctab[k] = cosine
        stab[k] = sine

    for copy in z_copies:
        copy.wait_recv()
    total = zbuf[0]
    for k in range(1, nz):
        total = total + zbuf[k]
    ybuf[0] = total
    y_copies = exchange(ybuf.at[0], ybuf, ny, y_peer, 16)

    for copy in tok_copies:
        copy.wait_recv()

    def norm_rows(i, carry):
        v = gtok[i].astype(F32)
        scaled = v * lax.rsqrt(jnp.mean(v * v, axis=1, keepdims=True) + EPS) * gain_row
        nv[pl.ds(pl.multiple_of(i * rows, rows), rows), :] = scaled
        return carry

    lax.fori_loop(0, ntp, norm_rows, 0)

    for copy in y_copies:
        copy.wait_recv()
    total = ybuf[0]
    for k in range(1, ny):
        total = total + ybuf[k]
    tbuf[tp] = total
    t_copies = []
    for k in range(1, ntp):
        t_copies.append(
            pltpu.make_async_remote_copy(
                src_ref=tbuf.at[tp],
                dst_ref=tbuf.at[tp],
                send_sem=send_sem.at[24 + k],
                recv_sem=recv_sem.at[24 + k],
                device_id=t_peer(k),
                device_id_type=MESH,
            )
        )
    for copy in t_copies:
        copy.start()
    for i in range(12, 16):
        loads[i].wait()
    for copy in t_copies:
        copy.wait_recv()

    def vector(which, who):
        return jnp.concatenate(
            [tbuf[t][who : who + 1, which * piece : (which + 1) * piece] for t in range(ntp)],
            axis=1,
        )

    shift_row = vector(0, 0)
    scale_row = 1.0 + vector(1, 0)

    def modulate(i, carry):
        at = pl.ds(pl.multiple_of(i * 16, 16), 16)
        hid[at, :] = (nv[at, :] * scale_row + shift_row).astype(BF16)
        return carry

    lax.fori_loop(0, LANES // 16, modulate, 0)
    ctx_hidden = nvc[...] * (1.0 + vector(1, 1)) + vector(0, 1)
    hid[LANES : LANES + 16, :] = jnp.concatenate(
        [ctx_hidden, jnp.zeros((16 - crow, width), F32)], axis=0
    ).astype(BF16)

    raw = jnp.dot(hid[...], wdown[...], preferred_element_type=F32)
    lat = raw * lax.rsqrt(jnp.mean(raw * raw, axis=1, keepdims=True) + EPS) * kvgain[...]
    rope = jnp.dot(hid[...], wrope[...], preferred_element_type=F32)
    rope = jnp.concatenate([rope, jnp.zeros((hid.shape[0], LANES - ROPE), F32)], axis=1)
    rope_t = rope[:LANES].T[:ROPE]
    ctx_lat = lat[LANES : LANES + crow]
    msg[0, 0, 0:64, :] = lat[0:64].astype(BF16)
    msg[0, 1, 0:64, :] = lat[64:128].astype(BF16)
    msg[0, 0, 64:80, 0:LANES] = rope_t[:16].astype(BF16)
    msg[0, 1, 64:80, 0:LANES] = rope_t[16:].astype(BF16)
    msg[0, 0, 64:80, LANES:] = jnp.concatenate([ctx_lat[:, :LANES], ctx_lat[:, LANES:]], axis=0).astype(BF16)
    msg[0, 1, 64:80, LANES:] = rope[LANES : LANES + 16].astype(BF16)
    k_copies = []
    for k in range(1, nz):
        k_copies.append(
            pltpu.make_async_remote_copy(
                src_ref=msg.at[0, core],
                dst_ref=msg.at[k, core],
                send_sem=send_sem.at[32 + k],
                recv_sem=recv_sem.at[32 + k],
                device_id=z_peer(k),
                device_id_type=MESH,
            )
        )
    for copy in k_copies:
        copy.start()

    raw = jnp.dot(hid[:LANES, :], wq[...], preferred_element_type=F32)
    raw_t = jnp.concatenate([raw, jnp.zeros((LANES, 2 * LANES - 2 * QK), F32)], axis=1).T
    plains, tails = [], []
    for h in range(2):
        u = raw_t[h * QK : (h + 1) * QK]
        inv = lax.rsqrt(jnp.sum(u * u, axis=0, keepdims=True) * (1.0 / QK) + EPS)
        u = u * inv * qg[:QK]
        plains.append(u[:HD])
        tails.append(rotated(u[HD:], ctab[0], stab[0]))
    plain = jnp.concatenate(plains, axis=0).T
    tail = jnp.concatenate(tails, axis=0)
    tail = jnp.concatenate([tail, pltpu.roll(tail, LANES // 2, 1)], axis=0).T
    qbuf[0, 0:LANES, :] = plain.astype(BF16)
    qbuf[0, LANES:, :] = tail[: LANES // 2].astype(BF16)
    q_copies = exchange(qbuf.at[0], qbuf, ny, y_peer, 40)

    def expand_slot(k):
        latent = msg[k, :, 0:64, :].reshape(LANES, KVL)
        rope_k = jnp.concatenate([msg[k, 0, 64:80, 0:LANES], msg[k, 1, 64:80, 0:LANES]], axis=0).astype(F32)
        up = nt_dot(wupt[...], latent)
        shared = jnp.sum(rope_k * rope_k, axis=0, keepdims=True)
        at = pl.ds(k * LANES, LANES)
        for h in range(2):
            part = up[h * HD : (h + 1) * HD]
            inv = lax.rsqrt((jnp.sum(part * part, axis=0, keepdims=True) + shared) * (1.0 / QK) + EPS)
            keys[h, h * HD : (h + 1) * HD, at] = (part * inv * kg[:HD]).astype(BF16)
            turned = rotated(rope_k * inv * kg[HD:QK], ctab[k], stab[k])
            keys[h, LANES + h * ROPE : LANES + (h + 1) * ROPE, at] = turned.astype(BF16)
        value = jnp.dot(latent, wup[1], preferred_element_type=F32)
        low = lane_ids((LANES, LANES)) < HD
        vals[0, at, :] = jnp.where(low, value, 1.0).astype(BF16)
        vals[1, at, :] = jnp.where(low, 1.0, value).astype(BF16)
        ctx_two = msg[k, 0, 64:80, LANES:].astype(F32)
        ctxl[k * crow : (k + 1) * crow, :] = jnp.concatenate([ctx_two[:crow], ctx_two[8 : 8 + crow]], axis=1)
        ctxr[k * crow : (k + 1) * crow, :] = msg[k, 1, 64:80, LANES:].astype(F32)[:crow]

    expand_slot(0)
    forwards = []
    for k in range(1, nz):
        k_copies[k - 1].wait_recv()
        forward = pltpu.make_async_remote_copy(
            src_ref=msg.at[k, core],
            dst_ref=msg.at[k, core],
            send_sem=fwd_send.at[k],
            recv_sem=fwd_recv.at[k],
            device_id=sibling,
            device_id_type=MESH,
        )
        forward.start()
        forwards.append(forward)
        if k > 1:
            forwards[k - 2].wait_recv()
            expand_slot(k - 1)
    forwards[nz - 2].wait_recv()
    expand_slot(nz - 1)

    latent = ctxl[...].astype(BF16)
    rope_k = ctxr[...].T[:ROPE]
    up = nt_dot(wupt[...], latent)
    shared = jnp.sum(rope_k * rope_k, axis=0, keepdims=True)
    at = pl.ds(nlat, LANES)
    for h in range(2):
        part = up[h * HD : (h + 1) * HD]
        inv = lax.rsqrt((jnp.sum(part * part, axis=0, keepdims=True) + shared) * (1.0 / QK) + EPS)
        keys[h, h * HD : (h + 1) * HD, at] = (part * inv * kg[:HD]).astype(BF16)
        keys[h, LANES + h * ROPE : LANES + (h + 1) * ROPE, at] = (rope_k * inv * kg[HD:QK]).astype(BF16)
    value = jnp.dot(latent, wup[1], preferred_element_type=F32)
    low = lane_ids((LANES, LANES)) < HD
    real = row_ids((LANES, LANES)) < nz * crow
    ones = jnp.where(real, 1.0, 0.0)
    vals[0, at, :] = jnp.where(low, value, ones).astype(BF16)
    vals[1, at, :] = jnp.where(low, ones, value).astype(BF16)

    for copy in q_copies:
        copy.wait_recv()
    lifts = [lift_s[0, h] * LOG2E for h in range(2)]
    diagonal = lane_ids((LANES, LANES)) % HD == row_ids((LANES, LANES)) % HD

    def attend(j, carry):
        tails = qbuf[j, LANES:, :]
        turned_tails = pltpu.roll(tails.astype(F32), LANES // 2, 1).astype(BF16)
        q = jnp.concatenate([qbuf[j, 0:LANES, :], jnp.concatenate([tails, turned_tails], axis=0)], axis=1)
        outs = []
        for h in range(2):
            acc = jnp.zeros((LANES, LANES), F32)
            for start in range(0, nlat + LANES, 256):
                size = min(256, nlat + LANES - start)
                s = jnp.dot(q, keys[h, :, start : start + size], preferred_element_type=F32)
                if start < nlat:
                    s = s - lifts[h]
                p = jnp.exp2(s).astype(BF16)
                acc = acc + jnp.dot(p, vals[h, start : start + size, :], preferred_element_type=F32)
            outs.append(acc)
        low = lane_ids((LANES, LANES)) < HD
        num = jnp.where(low, outs[0], outs[1])
        den = jnp.where(low, outs[1], outs[0])
        den = jnp.where(diagonal, den, 0.0)
        packed = jnp.concatenate(
            [
                jnp.sum(den[:HD], axis=0, keepdims=True),
                jnp.sum(den[HD:], axis=0, keepdims=True),
            ],
            axis=0,
        )
        hi = packed.astype(BF16).astype(F32)
        lo = packed - hi
        ostage[j, 0:LANES, :] = num.astype(BF16)
        ostage[j, LANES:, :] = jnp.concatenate([hi, lo, jnp.zeros((12, LANES), F32)], axis=0).astype(BF16)
        return carry

    o_copies = []
    for j in [k for k in range(1, ny)] + [0]:
        attend(j, 0)
        if j:
            copy = pltpu.make_async_remote_copy(
                src_ref=ostage.at[j],
                dst_ref=obuf.at[j],
                send_sem=send_sem.at[48 + j],
                recv_sem=recv_sem.at[48 + j],
                device_id=y_peer(ny - j),
                device_id_type=MESH,
            )
            copy.start()
            o_copies.append(copy)
    for copy in o_copies:
        copy.wait_recv()
    num = ostage[0, 0:LANES, :].astype(F32)
    den = ostage[0, LANES:, :].astype(F32)
    for j in range(1, ny):
        num = num + obuf[j, 0:LANES, :].astype(F32)
        den = den + obuf[j, LANES:, :].astype(F32)
    den = den[0:2] + den[2:4]
    spread = jnp.concatenate(
        [
            jnp.broadcast_to(den[0:1], (HD, LANES)),
            jnp.broadcast_to(den[1:2], (HD, LANES)),
        ],
        axis=0,
    )
    spread = jnp.where(diagonal, spread, 0.0)
    swap = jnp.where((lane_ids((LANES, LANES)) < HD) != (row_ids((LANES, LANES)) < HD), 1.0, 0.0)
    spread = jnp.dot(spread, swap, precision=HIGHEST, preferred_element_type=F32)
    attended = (num / spread).astype(BF16)

    proj = jnp.dot(attended, wout[...], preferred_element_type=F32).astype(BF16)
    for t in range(ntp):
        rstage[t] = proj[t * rows : (t + 1) * rows]
    r_copies = []
    for k in range(1, ntp):
        r_copies.append(
            pltpu.make_async_remote_copy(
                src_ref=rstage.at[(tp + k) % ntp],
                dst_ref=rbuf.at[k],
                send_sem=send_sem.at[56 + k],
                recv_sem=recv_sem.at[56 + k],
                device_id=t_peer(k),
                device_id_type=MESH,
            )
        )
    for copy in r_copies:
        copy.start()
    result = rstage[tp].astype(F32)
    for copy in r_copies:
        copy.wait_recv()
    for k in range(1, ntp):
        result = result + rbuf[k].astype(F32)
    out_ref[...] = (gtok[tp].astype(F32) + vector(2, 0) * result).astype(BF16)

    for copy in z_copies + tok_copies + y_copies + t_copies + k_copies + q_copies + forwards + o_copies + r_copies:
        copy.wait_send()


def solution(mesh, nz=8):
    nsp, ntp = mesh.shape["sp"], mesh.shape["tp"]
    ny = nsp // nz

    def local(
        latent_tokens,
        context_tokens,
        cond,
        ctx_cond,
        mod_shift,
        mod_scale,
        mod_gate,
        norm_gain,
        w_query,
        query_gain,
        w_down_kv,
        w_rope_key,
        kv_gain,
        w_up_kv,
        key_gain,
        ctx_lift,
        w_output,
    ):
        rows, width = latent_tokens.shape
        crow = context_tokens.shape[0]
        piece = mod_shift.shape[1]
        lat = nz * LANES
        vm = pltpu.VMEM
        anywhere = pl.BlockSpec(memory_space=pl.ANY)
        smem = pl.BlockSpec(memory_space=pltpu.SMEM)
        return pl.pallas_call(
            functools.partial(kernel, nz, ny, ntp),
            out_shape=jax.ShapeDtypeStruct((rows, width), BF16),
            in_specs=[anywhere] * 15 + [smem, anywhere],
            out_specs=pl.BlockSpec(memory_space=pltpu.VMEM),
            scratch_shapes=[
                vm((ntp, rows, width), BF16),
                vm((crow, width), BF16),
                vm((width // LANES, LANES), F32),
                vm((width // LANES, LANES), F32),
                vm((3, mod_shift.shape[0], piece), BF16),
                vm((1, width), F32),
                vm(w_query.shape, BF16),
                vm((1, QK), F32),
                vm(w_down_kv.shape, BF16),
                vm(w_rope_key.shape, BF16),
                vm((1, KVL), F32),
                vm(w_up_kv.shape, BF16),
                vm((1, QK), F32),
                vm(w_output.shape, BF16),
                vm((nz, 2, 3 * piece), F32),
                vm((ny, 2, 3 * piece), F32),
                vm((ntp, 2, 3 * piece), F32),
                vm((LANES, width), F32),
                vm((crow, width), F32),
                vm((LANES + 16, width), BF16),
                vm((LANES, KVL), BF16),
                vm((nz, HALF, LANES), F32),
                vm((nz, HALF, LANES), F32),
                vm((nz, 2, MSG, KVL), BF16),
                vm((ny, LANES + HD, LANES), BF16),
                vm((8, LANES), F32),
                vm((2, 2 * LANES, lat + LANES), BF16),
                vm((2, lat + LANES, LANES), BF16),
                vm((LANES, KVL), F32),
                vm((LANES, LANES), F32),
                vm((ny, LANES + 16, LANES), BF16),
                vm((ny, LANES + 16, LANES), BF16),
                vm((ntp, rows, width), BF16),
                vm((ntp, rows, width), BF16),
                pltpu.SemaphoreType.DMA((16,)),
                pltpu.SemaphoreType.DMA((64,)),
                pltpu.SemaphoreType.DMA((64,)),
                pltpu.SemaphoreType.DMA((8,)),
                pltpu.SemaphoreType.DMA((8,)),
            ],
            compiler_params=pltpu.CompilerParams(
                collective_id=0, has_side_effects=True, vmem_limit_bytes=60 * 1024 * 1024
            ),
        )(
            latent_tokens,
            context_tokens,
            cond.reshape(width // LANES, LANES),
            ctx_cond.reshape(width // LANES, LANES),
            mod_shift,
            mod_scale,
            mod_gate,
            norm_gain.reshape(1, width),
            w_query,
            query_gain.reshape(1, QK),
            w_down_kv,
            w_rope_key,
            kv_gain.reshape(1, KVL),
            w_up_kv,
            key_gain.reshape(1, QK),
            ctx_lift.reshape(1, 2),
            w_output,
        )

    in_specs = (
        P(("sp", "tp"), None),
        P("sp", None),
        P(),
        P(),
        P("sp", "tp"),
        P("sp", "tp"),
        P("sp", "tp"),
        P(),
        P(None, "tp"),
        P(),
        P(),
        P(),
        P(),
        P(None, None, "tp"),
        P(),
        P("tp"),
        P("tp", None),
    )
    return jax.shard_map(local, mesh=mesh, in_specs=in_specs, out_specs=P(("sp", "tp"), None), check_vma=False)
```

time: 227 us -> 71.5 us (0.31)
  waiting for transfers between devices: 108 us -> 0 us
  blocking collectives: 74.6 us -> 0 us
  Pallas kernels: 0 us -> 65.7 us
  between operations: 13.7 us -> 0.01 us
  matrix products: 12.7 us -> 0 us
  other arithmetic: 8.28 us -> 0 us
  starting transfers between devices: 3.9 us -> 0 us
    all_gather x2 -> x0, waiting for transfers between devices: 98.7 us -> none  [the longest x1 88.4 us: in_one_piece(): lax.all_gather(both, axis, axis=dim, tiled=True)]
    pallas_call x0 -> x1, Pallas kernels: none -> 65.7 us  [local(): pl.pallas_call(functools.partial(kernel, nz, ny, ntp), out_shape=jax.Shap...]
    psum x2 -> x0, blocking collectives: 35.2 us -> none  [over_axes(): return functools.reduce(lax.psum, axes, value)]
    all_gather x1 -> x0, blocking collectives: 20.5 us -> none  [in_one_piece(): lax.all_gather(both, axis, axis=dim, tiled=True)]
    all_to_all x1 -> x0, blocking collectives: 18.9 us -> none  [sent_and_summed(): tiles = lax.all_to_all(split_up(value, dim, count), axis, 0, 0, tiled=True)]
    dot_general x17 -> x0, matrix products: 12.7 us -> none  [the longest x2 3.3 us: compress(): jnp.dot(hidden, w_down_kv, preferred_element_type=jnp.float32)]
    all_to_all x1 -> x0, waiting for transfers between devices: 8.21 us -> none  [copy_for_each(): return lax.all_to_all(copies, axis, split_axis=0, concat_axis=0, tiled=True)]
    unnamed x24 -> x3, local copies, waits for them, and re-layouts: 0.08 us -> 5.63 us
  transfers between devices with their start and end apart: 3 -> 0, of which waited for: 3 -> 0; matrix products, arithmetic and copies ran while one was open for 7% -> 0% of each run, Pallas kernels for 0% -> 0%
where the time goes in v1:
time: 71.5 us; the launch traced here: 71.3 us
  Pallas kernels  65.7 us (92%)
  local copies, waits for them, and re-layouts  5.63 us (8%)
    pallas_call x1, Pallas kernels, local(): pl.pallas_call(functools.partial(kernel, nz, ny, ntp), out_shape=jax.Shap...  65.7 us
    unnamed x3, local copies, waits for them, and re-layouts  5.63 us

profile of v1, /device:TPU:1, one launch (start us, length us, event | category | flops | bytes accessed | tf_op | source)
XLA Modules:
  0.0 71.3 jit_solution(16167919739970159000)
XLA Ops:
  0.0 1.9 %copy.19.wrope_h = bf16[2048,32]{1,0:T(8,128)(2,1)} copy(bf16[2048,32]{0,1:T(8,128)(2,1)} %param.28) | data formatting | bytes 262144 | tf_op args[11]
  1.9 2.2 %copy.18.wq_h = bf16[2048,192]{1,0:T(8,128)(2,1)} copy(bf16[2048,192]{0,1:T(8,128)(2,1)} %param.25) | data formatting | bytes 1572864 | tf_op args[8]
  4.2 65.7 %shard_map.163 = bf16[16,2048]{1,0:T(8,128)(2,1)} custom-call(bf16[16,2048]{1,0:T(8,128)(2,1)} %tok_h.1, bf16[8,2048]{1,0:T(8,128)(2,1)} %ctx_h.1, f32[16,128]{1,0:T(8,128)} %bitcast.7, f32[16,128]{1,0:T(8,128)} %bitcast.8, bf16[32,256]{1,0:T(8,128)(2,1)} %mshift_h.1, bf16[32,256]{1,0:T(8,128)(2,1)} %mscale_h.1, bf16[32,256]{1,0:T(8,128)(2,1)} %mgate_h.1, ...), custom_call_target="tpu_custom_call" | custom-call | tf_op jit(solution)/shard_map/pallas_call | solution.py:549
  69.8 1.5 %copy.21 = bf16[16,2048]{1,0:T(8,128)(2,1)} copy(bf16[16,2048]{1,0:T(8,128)(2,1)} %shard_map.163) | data formatting | bytes 131072

commit v2 on v1

--- a/solution.py
+++ b/solution.py
@@ -104,6 +104,9 @@
     zbuf,
     ybuf,
     tbuf,
+    gzbuf,
+    gybuf,
+    gtbuf,
     nv,
     nvc,
     hid,
@@ -112,7 +115,6 @@
     stab,
     msg,
     qbuf,
-    qfull,
     keys,
     vals,
     ctxl,
@@ -195,44 +197,8 @@
     block = jnp.concatenate([mods[0], mods[1], mods[2]], axis=1).astype(F32)
     block = jnp.concatenate([block] * fold, axis=0)
     share = jnp.dot(signal, block, precision=HIGHEST, preferred_element_type=F32)
-    zbuf[0] = share[0:2]
-
-    pl.semaphore_wait(barrier, len(peers))
-
-    def exchange(src, buf, count, peer, first):
-        copies = []
-        for k in range(1, count):
-            copies.append(
-                pltpu.make_async_remote_copy(
-                    src_ref=src,
-                    dst_ref=buf.at[k],
-                    send_sem=send_sem.at[first + k],
-                    recv_sem=recv_sem.at[first + k],
-                    device_id=peer(k),
-                    device_id_type=MESH,
-                )
-            )
-        for copy in copies:
-            copy.start()
-        return copies
-
-    z_copies = exchange(zbuf.at[0], zbuf, nz, z_peer, 0)
-
-    loads[5].wait()
-    tok_copies = []
-    for k in range(1, ntp):
-        tok_copies.append(
-            pltpu.make_async_remote_copy(
-                src_ref=gtok.at[tp],
-                dst_ref=gtok.at[tp],
-                send_sem=send_sem.at[8 + k],
-                recv_sem=recv_sem.at[8 + k],
-                device_id=t_peer(k),
-                device_id_type=MESH,
-            )
-        )
-    for copy in tok_copies:
-        copy.start()
+    zbuf[0] = share[0:2, : 2 * piece]
+    gzbuf[0] = share[0:1, 2 * piece :]
 
     for i in range(6, 12):
         loads[i].wait()
@@ -253,6 +219,49 @@
         ctab[k] = cosine
         stab[k] = sine
 
+
+    pl.semaphore_wait(barrier, len(peers))
+
+    def near_first(count):
+        return sorted(range(1, count), key=lambda k: min(k, count - k))
+
+    def exchange(src, buf, count, peer, first, near=False):
+        copies = []
+        for k in range(1, count):
+            copies.append(
+                pltpu.make_async_remote_copy(
+                    src_ref=src,
+                    dst_ref=buf.at[k],
+                    send_sem=send_sem.at[first + k],
+                    recv_sem=recv_sem.at[first + k],
+                    device_id=peer(k),
+                    device_id_type=MESH,
+                )
+            )
+        order = near_first(count)
+        for k in order if near else order[::-1]:
+            copies[k - 1].start()
+        return copies
+
+    z_copies = exchange(zbuf.at[0], zbuf, nz, z_peer, 0)
+    gz_copies = exchange(gzbuf.at[0], gzbuf, nz, z_peer, 64)
+
+    loads[5].wait()
+    tok_copies = []
+    for k in range(1, ntp):
+        tok_copies.append(
+            pltpu.make_async_remote_copy(
+                src_ref=gtok.at[tp],
+                dst_ref=gtok.at[tp],
+                send_sem=send_sem.at[8 + k],
+                recv_sem=recv_sem.at[8 + k],
+                device_id=t_peer(k),
+                device_id_type=MESH,
+            )
+        )
+    for copy in tok_copies:
+        copy.start()
+
     for copy in z_copies:
         copy.wait_recv()
     total = zbuf[0]
@@ -260,6 +269,13 @@
         total = total + zbuf[k]
     ybuf[0] = total
     y_copies = exchange(ybuf.at[0], ybuf, ny, y_peer, 16)
+    for copy in gz_copies:
+        copy.wait_recv()
+    total = gzbuf[0]
+    for k in range(1, nz):
+        total = total + gzbuf[k]
+    gybuf[0] = total
+    gy_copies = exchange(gybuf.at[0], gybuf, ny, y_peer, 72)
 
     for copy in tok_copies:
         copy.wait_recv()
@@ -278,20 +294,32 @@
     for k in range(1, ny):
         total = total + ybuf[k]
     tbuf[tp] = total
-    t_copies = []
-    for k in range(1, ntp):
-        t_copies.append(
-            pltpu.make_async_remote_copy(
-                src_ref=tbuf.at[tp],
-                dst_ref=tbuf.at[tp],
-                send_sem=send_sem.at[24 + k],
-                recv_sem=recv_sem.at[24 + k],
-                device_id=t_peer(k),
-                device_id_type=MESH,
+
+    def spread_tp(buf, first):
+        copies = []
+        for k in range(1, ntp):
+            copies.append(
+                pltpu.make_async_remote_copy(
+                    src_ref=buf.at[tp],
+                    dst_ref=buf.at[tp],
+                    send_sem=send_sem.at[first + k],
+                    recv_sem=recv_sem.at[first + k],
+                    device_id=t_peer(k),
+                    device_id_type=MESH,
+                )
             )
-        )
-    for copy in t_copies:
-        copy.start()
+        for copy in copies:
+            copy.start()
+        return copies
+
+    t_copies = spread_tp(tbuf, 24)
+    for copy in gy_copies:
+        copy.wait_recv()
+    total = gybuf[0]
+    for k in range(1, ny):
+        total = total + gybuf[k]
+    gtbuf[tp] = total
+    gt_copies = spread_tp(gtbuf, 80)
     for i in range(12, 16):
         loads[i].wait()
     for copy in t_copies:
@@ -319,16 +347,16 @@
 
     raw = jnp.dot(hid[...], wdown[...], preferred_element_type=F32)
     lat = raw * lax.rsqrt(jnp.mean(raw * raw, axis=1, keepdims=True) + EPS) * kvgain[...]
-    rope = jnp.dot(hid[...], wrope[...], preferred_element_type=F32)
-    rope = jnp.concatenate([rope, jnp.zeros((hid.shape[0], LANES - ROPE), F32)], axis=1)
-    rope_t = rope[:LANES].T[:ROPE]
+    rope_t = nt_dot(wrope[...], hid[:LANES, :])
+    rope_c = nt_dot(hid[LANES:, :], wrope[...])
+    rope_c = jnp.concatenate([rope_c, jnp.zeros((16, LANES - ROPE), F32)], axis=1)
     ctx_lat = lat[LANES : LANES + crow]
     msg[0, 0, 0:64, :] = lat[0:64].astype(BF16)
     msg[0, 1, 0:64, :] = lat[64:128].astype(BF16)
     msg[0, 0, 64:80, 0:LANES] = rope_t[:16].astype(BF16)
     msg[0, 1, 64:80, 0:LANES] = rope_t[16:].astype(BF16)
     msg[0, 0, 64:80, LANES:] = jnp.concatenate([ctx_lat[:, :LANES], ctx_lat[:, LANES:]], axis=0).astype(BF16)
-    msg[0, 1, 64:80, LANES:] = rope[LANES : LANES + 16].astype(BF16)
+    msg[0, 1, 64:80, LANES:] = rope_c.astype(BF16)
     k_copies = []
     for k in range(1, nz):
         k_copies.append(
@@ -341,11 +369,10 @@
                 device_id_type=MESH,
             )
         )
-    for copy in k_copies:
-        copy.start()
-
-    raw = jnp.dot(hid[:LANES, :], wq[...], preferred_element_type=F32)
-    raw_t = jnp.concatenate([raw, jnp.zeros((LANES, 2 * LANES - 2 * QK), F32)], axis=1).T
+    for k in near_first(nz):
+        k_copies[k - 1].start()
+
+    raw_t = nt_dot(wq[...], hid[:LANES, :])
     plains, tails = [], []
     for h in range(2):
         u = raw_t[h * QK : (h + 1) * QK]
@@ -358,7 +385,7 @@
     tail = jnp.concatenate([tail, pltpu.roll(tail, LANES // 2, 1)], axis=0).T
     qbuf[0, 0:LANES, :] = plain.astype(BF16)
     qbuf[0, LANES:, :] = tail[: LANES // 2].astype(BF16)
-    q_copies = exchange(qbuf.at[0], qbuf, ny, y_peer, 40)
+    q_copies = exchange(qbuf.at[0], qbuf, ny, y_peer, 40, near=True)
 
     def expand_slot(k):
         latent = msg[k, :, 0:64, :].reshape(LANES, KVL)
@@ -382,7 +409,8 @@
 
     expand_slot(0)
     forwards = []
-    for k in range(1, nz):
+    passed = []
+    for k in near_first(nz):
         k_copies[k - 1].wait_recv()
         forward = pltpu.make_async_remote_copy(
             src_ref=msg.at[k, core],
@@ -394,11 +422,12 @@
         )
         forward.start()
         forwards.append(forward)
-        if k > 1:
-            forwards[k - 2].wait_recv()
-            expand_slot(k - 1)
-    forwards[nz - 2].wait_recv()
-    expand_slot(nz - 1)
+        passed.append(k)
+        if len(passed) > 1:
+            forwards[-2].wait_recv()
+            expand_slot(passed[-2])
+    forwards[-1].wait_recv()
+    expand_slot(passed[-1])
 
     latent = ctxl[...].astype(BF16)
     rope_k = ctxr[...].T[:ROPE]
@@ -417,47 +446,49 @@
     vals[0, at, :] = jnp.where(low, value, ones).astype(BF16)
     vals[1, at, :] = jnp.where(low, ones, value).astype(BF16)
 
-    for copy in q_copies:
-        copy.wait_recv()
-    lifts = [lift_s[0, h] * LOG2E for h in range(2)]
     diagonal = lane_ids((LANES, LANES)) % HD == row_ids((LANES, LANES)) % HD
 
-    def attend(j, carry):
+    low = lane_ids((LANES, LANES)) < HD
+    late = lane_ids((1, nlat + LANES)) < nlat
+    lifts = [jnp.where(late, lift_s[0, h] * LOG2E, 0.0) for h in range(2)]
+
+    def whole_query(j):
         tails = qbuf[j, LANES:, :]
         turned_tails = pltpu.roll(tails.astype(F32), LANES // 2, 1).astype(BF16)
-        q = jnp.concatenate([qbuf[j, 0:LANES, :], jnp.concatenate([tails, turned_tails], axis=0)], axis=1)
+        return jnp.concatenate([qbuf[j, 0:LANES, :], jnp.concatenate([tails, turned_tails], axis=0)], axis=1)
+
+    def attend(slots):
+        q = jnp.concatenate([whole_query(j) for j in slots], axis=0)
         outs = []
         for h in range(2):
-            acc = jnp.zeros((LANES, LANES), F32)
-            for start in range(0, nlat + LANES, 256):
-                size = min(256, nlat + LANES - start)
-                s = jnp.dot(q, keys[h, :, start : start + size], preferred_element_type=F32)
-                if start < nlat:
-                    s = s - lifts[h]
-                p = jnp.exp2(s).astype(BF16)
-                acc = acc + jnp.dot(p, vals[h, start : start + size, :], preferred_element_type=F32)
-            outs.append(acc)
-        low = lane_ids((LANES, LANES)) < HD
-        num = jnp.where(low, outs[0], outs[1])
-        den = jnp.where(low, outs[1], outs[0])
-        den = jnp.where(diagonal, den, 0.0)
-        packed = jnp.concatenate(
-            [
-                jnp.sum(den[:HD], axis=0, keepdims=True),
-                jnp.sum(den[HD:], axis=0, keepdims=True),
-            ],
-            axis=0,
-        )
-        hi = packed.astype(BF16).astype(F32)
-        lo = packed - hi
-        ostage[j, 0:LANES, :] = num.astype(BF16)
-        ostage[j, LANES:, :] = jnp.concatenate([hi, lo, jnp.zeros((12, LANES), F32)], axis=0).astype(BF16)
-        return carry
+            p = jnp.exp2(jnp.dot(q, keys[h], preferred_element_type=F32) - lifts[h]).astype(BF16)
+            outs.append(jnp.dot(p, vals[h], preferred_element_type=F32))
+        for i, j in enumerate(slots):
+            first, second = (out[i * LANES : (i + 1) * LANES] for out in outs)
+            den = jnp.where(diagonal, jnp.where(low, second, first), 0.0)
+            packed = jnp.concatenate(
+                [
+                    jnp.sum(den[:HD], axis=0, keepdims=True),
+                    jnp.sum(den[HD:], axis=0, keepdims=True),
+                ],
+                axis=0,
+            )
+            hi = packed.astype(BF16).astype(F32)
+            lo = packed - hi
+            ostage[j, 0:LANES, :] = jnp.where(low, first, second).astype(BF16)
+            ostage[j, LANES:, :] = jnp.concatenate([hi, lo, jnp.zeros((12, LANES), F32)], axis=0).astype(BF16)
 
     o_copies = []
-    for j in [k for k in range(1, ny)] + [0]:
-        attend(j, 0)
-        if j:
+    order = sorted(range(ny), key=lambda j: min(j, ny - j))
+    for at in range(0, ny, 2):
+        slots = order[at : at + 2]
+        for j in slots:
+            if j:
+                q_copies[j - 1].wait_recv()
+        attend(slots)
+        for j in slots:
+            if j == 0:
+                continue
             copy = pltpu.make_async_remote_copy(
                 src_ref=ostage.at[j],
                 dst_ref=obuf.at[j],
@@ -510,9 +541,12 @@
         copy.wait_recv()
     for k in range(1, ntp):
         result = result + rbuf[k].astype(F32)
-    out_ref[...] = (gtok[tp].astype(F32) + vector(2, 0) * result).astype(BF16)
-
-    for copy in z_copies + tok_copies + y_copies + t_copies + k_copies + q_copies + forwards + o_copies + r_copies:
+    for copy in gt_copies:
+        copy.wait_recv()
+    gate_row = jnp.concatenate([gtbuf[t] for t in range(ntp)], axis=1)
+    out_ref[...] = (gtok[tp].astype(F32) + gate_row * result).astype(BF16)
+
+    for copy in gz_copies + gy_copies + gt_copies + z_copies + tok_copies + y_copies + t_copies + k_copies + q_copies + forwards + o_copies + r_copies:
         copy.wait_send()
 
 
@@ -558,17 +592,20 @@
                 vm((width // LANES, LANES), F32),
                 vm((3, mod_shift.shape[0], piece), BF16),
                 vm((1, width), F32),
-                vm(w_query.shape, BF16),
+                vm(w_query.shape[::-1], BF16),
                 vm((1, QK), F32),
                 vm(w_down_kv.shape, BF16),
-                vm(w_rope_key.shape, BF16),
+                vm(w_rope_key.shape[::-1], BF16),
                 vm((1, KVL), F32),
                 vm(w_up_kv.shape, BF16),
                 vm((1, QK), F32),
                 vm(w_output.shape, BF16),
-                vm((nz, 2, 3 * piece), F32),
-                vm((ny, 2, 3 * piece), F32),
-                vm((ntp, 2, 3 * piece), F32),
+                vm((nz, 2, 2 * piece), F32),
+                vm((ny, 2, 2 * piece), F32),
+                vm((ntp, 2, 2 * piece), F32),
+                vm((nz, 1, piece), F32),
+                vm((ny, 1, piece), F32),
+                vm((ntp, 1, piece), F32),
                 vm((LANES, width), F32),
                 vm((crow, width), F32),
                 vm((LANES + 16, width), BF16),
@@ -577,7 +614,6 @@
                 vm((nz, HALF, LANES), F32),
                 vm((nz, 2, MSG, KVL), BF16),
                 vm((ny, LANES + HD, LANES), BF16),
-                vm((8, LANES), F32),
                 vm((2, 2 * LANES, lat + LANES), BF16),
                 vm((2, lat + LANES, LANES), BF16),
                 vm((LANES, KVL), F32),
@@ -587,8 +623,8 @@
                 vm((ntp, rows, width), BF16),
                 vm((ntp, rows, width), BF16),
                 pltpu.SemaphoreType.DMA((16,)),
-                pltpu.SemaphoreType.DMA((64,)),
-                pltpu.SemaphoreType.DMA((64,)),
+                pltpu.SemaphoreType.DMA((96,)),
+                pltpu.SemaphoreType.DMA((96,)),
                 pltpu.SemaphoreType.DMA((8,)),
                 pltpu.SemaphoreType.DMA((8,)),
             ],
@@ -604,10 +640,10 @@
             mod_scale,
             mod_gate,
             norm_gain.reshape(1, width),
-            w_query,
+            w_query.T,
             query_gain.reshape(1, QK),
             w_down_kv,
-            w_rope_key,
+            w_rope_key.T,
             kv_gain.reshape(1, KVL),
             w_up_kv,
             key_gain.reshape(1, QK),

time: 71.5 us -> 63.3 us (0.89)
  Pallas kernels: 65.7 us -> 61.2 us
  local copies, waits for them, and re-layouts: 5.63 us -> 1.47 us
    pallas_call x1, Pallas kernels: 65.7 us -> 61.2 us  [local(): pl.pallas_call(functools.partial(kernel, nz, ny, ntp), out_shape=jax.Shap...]
    unnamed x3 -> x1, local copies, waits for them, and re-layouts: 5.63 us -> 1.47 us
where the time goes in v2:
time: 63.3 us; the launch traced here: 62.6 us
  Pallas kernels  61.2 us (97%)
  local copies, waits for them, and re-layouts  1.47 us (2%)
    pallas_call x1, Pallas kernels, local(): pl.pallas_call(functools.partial(kernel, nz, ny, ntp), out_shape=jax.Shap...  61.2 us
    unnamed x1, local copies, waits for them, and re-layouts  1.47 us

profile of v2, /device:TPU:1, one launch (start us, length us, event | category | flops | bytes accessed | tf_op | source)
XLA Modules:
  0.0 62.6 jit_solution(6980971979163461004)
XLA Ops:
  0.0 61.2 %shard_map.163 = bf16[16,2048]{1,0:T(8,128)(2,1)} custom-call(bf16[16,2048]{1,0:T(8,128)(2,1)} %tok_h.1, bf16[8,2048]{1,0:T(8,128)(2,1)} %ctx_h.1, f32[16,128]{1,0:T(8,128)} %bitcast.11, f32[16,128]{1,0:T(8,128)} %bitcast.12, bf16[32,256]{1,0:T(8,128)(2,1)} %mshift_h.1, bf16[32,256]{1,0:T(8,128)(2,1)} %mscale_h.1, bf16[32,256]{1,0:T(8,128)(2,1)} %mgate_h.1, ...), custom_call_target="tpu_custom_call" | custom-call | tf_op jit(solution)/shard_map/pallas_call | solution.py:583
  61.2 1.5 %copy.19 = bf16[16,2048]{1,0:T(8,128)(2,1)} copy(bf16[16,2048]{1,0:T(8,128)(2,1)} %shard_map.163) | data formatting | bytes 131072

commit v3 on v2

--- a/solution.py
+++ b/solution.py
@@ -45,6 +45,20 @@
     width = row.shape[1]
     full = jnp.concatenate([row, jnp.zeros((1, LANES - width), F32)], axis=1)
     return jnp.broadcast_to(full, (LANES, LANES)).T
+
+
+class Flight:
+    def __init__(self, sent, copy):
+        self.copy, self.landed = copy, False
+        sent.append(self)
+        copy.start()
+
+    def wait_recv(self):
+        self.landed = True
+        self.copy.wait_recv()
+
+    def wait_send(self):
+        self.copy.wait_send()
 
 
 def angle_tables(group):
@@ -121,13 +135,12 @@
     ctxr,
     ostage,
     obuf,
+    opass,
     rstage,
     rbuf,
     load_sem,
     send_sem,
     recv_sem,
-    fwd_send,
-    fwd_recv,
 ):
     sp = lax.axis_index("sp")
     tp = lax.axis_index("tp")
@@ -149,6 +162,12 @@
         return (sp, (tp + k) % ntp)
 
     sibling = (sp, tp + 1 - 2 * core)
+
+    def x_index(k):
+        return (tp + 2 * k) % ntp
+
+    def x_peer(k):
+        return (sp, x_index(k))
 
     pairs = [
         (cond_h, cond_v),
@@ -200,6 +219,50 @@
     zbuf[0] = share[0:2, : 2 * piece]
     gzbuf[0] = share[0:1, 2 * piece :]
 
+    pl.semaphore_wait(barrier, len(peers))
+
+    sent = []
+
+    def remote(src, dst, index, device):
+        return Flight(
+            sent,
+            pltpu.make_async_remote_copy(
+                src_ref=src,
+                dst_ref=dst,
+                send_sem=send_sem.at[index],
+                recv_sem=recv_sem.at[index],
+                device_id=device,
+                device_id_type=MESH,
+            ),
+        )
+
+    def far_first(count):
+        return sorted(range(1, count), key=lambda k: -min(k, count - k))
+
+    def exchange(buf, count, peer, first):
+        return [remote(buf.at[0], buf.at[k], first + k, peer(k)) for k in far_first(count)]
+
+    def spread_tp(buf, first):
+        return [remote(buf.at[tp], buf.at[tp], first + k, t_peer(k)) for k in range(1, ntp)]
+
+    def direct(count):
+        if count < 8:
+            return list(range(1, count))
+        return [2, count - 2, 1, count - 1]
+
+    def landed(flights):
+        for flight in flights:
+            flight.wait_recv()
+
+    z_copies = exchange(zbuf, nz, z_peer, 0)
+    gz_copies = exchange(gzbuf, nz, z_peer, 8)
+
+    loads[5].wait()
+    near_x = sorted({k for k in (1, ntp // 2 - 1) if 0 < k < ntp // 2})
+    tok_near = {k: remote(gtok.at[tp], gtok.at[tp], 16 + k, x_peer(k)) for k in near_x}
+    tok_side = [remote(gtok.at[tp], gtok.at[tp], 16, sibling)]
+    tok_half = []
+
     for i in range(6, 12):
         loads[i].wait()
     gain_row = ngain[...]
@@ -219,66 +282,48 @@
         ctab[k] = cosine
         stab[k] = sine
 
-
-    pl.semaphore_wait(barrier, len(peers))
-
-    def near_first(count):
-        return sorted(range(1, count), key=lambda k: min(k, count - k))
-
-    def exchange(src, buf, count, peer, first, near=False):
-        copies = []
-        for k in range(1, count):
-            copies.append(
-                pltpu.make_async_remote_copy(
-                    src_ref=src,
-                    dst_ref=buf.at[k],
-                    send_sem=send_sem.at[first + k],
-                    recv_sem=recv_sem.at[first + k],
-                    device_id=peer(k),
-                    device_id_type=MESH,
-                )
+    for k in near_x:
+        tok_near[k].wait_recv()
+        came = x_index(ntp // 2 - k)
+        if ntp // 2 == 4:
+            lanes = pl.ds(0 if k == 1 else width // 2, width // 2)
+            tok_half.append(
+                remote(gtok.at[came, :, lanes], gtok.at[came, :, lanes], 20 + k, x_peer(k))
             )
-        order = near_first(count)
-        for k in order if near else order[::-1]:
-            copies[k - 1].start()
-        return copies
-
-    z_copies = exchange(zbuf.at[0], zbuf, nz, z_peer, 0)
-    gz_copies = exchange(gzbuf.at[0], gzbuf, nz, z_peer, 64)
-
-    loads[5].wait()
-    tok_copies = []
-    for k in range(1, ntp):
-        tok_copies.append(
-            pltpu.make_async_remote_copy(
-                src_ref=gtok.at[tp],
-                dst_ref=gtok.at[tp],
-                send_sem=send_sem.at[8 + k],
-                recv_sem=recv_sem.at[8 + k],
-                device_id=t_peer(k),
-                device_id_type=MESH,
-            )
-        )
-    for copy in tok_copies:
-        copy.start()
-
-    for copy in z_copies:
-        copy.wait_recv()
+        tok_side.append(remote(gtok.at[came], gtok.at[came], 24 + k, sibling))
+
+    landed(z_copies)
     total = zbuf[0]
     for k in range(1, nz):
         total = total + zbuf[k]
     ybuf[0] = total
-    y_copies = exchange(ybuf.at[0], ybuf, ny, y_peer, 16)
-    for copy in gz_copies:
-        copy.wait_recv()
+    y_copies = exchange(ybuf, ny, y_peer, 32)
+    landed(gz_copies)
     total = gzbuf[0]
     for k in range(1, nz):
         total = total + gzbuf[k]
     gybuf[0] = total
-    gy_copies = exchange(gybuf.at[0], gybuf, ny, y_peer, 72)
-
-    for copy in tok_copies:
-        copy.wait_recv()
+    gy_copies = exchange(gybuf, ny, y_peer, 40)
+
+    if tok_half:
+        landed(tok_half)
+        far = x_index(2)
+        tok_side.append(remote(gtok.at[far], gtok.at[far], 28, sibling))
+    landed(y_copies)
+    total = ybuf[0]
+    for k in range(1, ny):
+        total = total + ybuf[k]
+    tbuf[tp] = total
+
+    t_copies = spread_tp(tbuf, 48)
+    landed(gy_copies)
+    total = gybuf[0]
+    for k in range(1, ny):
+        total = total + gybuf[k]
+    gtbuf[tp] = total
+    gt_copies = spread_tp(gtbuf, 56)
+
+    landed(tok_side)
 
     def norm_rows(i, carry):
         v = gtok[i].astype(F32)
@@ -288,42 +333,9 @@
 
     lax.fori_loop(0, ntp, norm_rows, 0)
 
-    for copy in y_copies:
-        copy.wait_recv()
-    total = ybuf[0]
-    for k in range(1, ny):
-        total = total + ybuf[k]
-    tbuf[tp] = total
-
-    def spread_tp(buf, first):
-        copies = []
-        for k in range(1, ntp):
-            copies.append(
-                pltpu.make_async_remote_copy(
-                    src_ref=buf.at[tp],
-                    dst_ref=buf.at[tp],
-                    send_sem=send_sem.at[first + k],
-                    recv_sem=recv_sem.at[first + k],
-                    device_id=t_peer(k),
-                    device_id_type=MESH,
-                )
-            )
-        for copy in copies:
-            copy.start()
-        return copies
-
-    t_copies = spread_tp(tbuf, 24)
-    for copy in gy_copies:
-        copy.wait_recv()
-    total = gybuf[0]
-    for k in range(1, ny):
-        total = total + gybuf[k]
-    gtbuf[tp] = total
-    gt_copies = spread_tp(gtbuf, 80)
     for i in range(12, 16):
         loads[i].wait()
-    for copy in t_copies:
-        copy.wait_recv()
+    landed(t_copies)
 
     def vector(which, who):
         return jnp.concatenate(
@@ -357,20 +369,9 @@
     msg[0, 1, 64:80, 0:LANES] = rope_t[16:].astype(BF16)
     msg[0, 0, 64:80, LANES:] = jnp.concatenate([ctx_lat[:, :LANES], ctx_lat[:, LANES:]], axis=0).astype(BF16)
     msg[0, 1, 64:80, LANES:] = rope_c.astype(BF16)
-    k_copies = []
-    for k in range(1, nz):
-        k_copies.append(
-            pltpu.make_async_remote_copy(
-                src_ref=msg.at[0, core],
-                dst_ref=msg.at[k, core],
-                send_sem=send_sem.at[32 + k],
-                recv_sem=recv_sem.at[32 + k],
-                device_id=z_peer(k),
-                device_id_type=MESH,
-            )
-        )
-    for k in near_first(nz):
-        k_copies[k - 1].start()
+    k_near = {
+        k: remote(msg.at[0, core], msg.at[k, core], 64 + k, z_peer(k)) for k in direct(nz)
+    }
 
     raw_t = nt_dot(wq[...], hid[:LANES, :])
     plains, tails = [], []
@@ -385,7 +386,7 @@
     tail = jnp.concatenate([tail, pltpu.roll(tail, LANES // 2, 1)], axis=0).T
     qbuf[0, 0:LANES, :] = plain.astype(BF16)
     qbuf[0, LANES:, :] = tail[: LANES // 2].astype(BF16)
-    q_copies = exchange(qbuf.at[0], qbuf, ny, y_peer, 40, near=True)
+    q_near = {k: remote(qbuf.at[0], qbuf.at[k], 80 + k, y_peer(k)) for k in direct(ny)}
 
     def expand_slot(k):
         latent = msg[k, :, 0:64, :].reshape(LANES, KVL)
@@ -408,26 +409,49 @@
         ctxr[k * crow : (k + 1) * crow, :] = msg[k, 1, 64:80, LANES:].astype(F32)[:crow]
 
     expand_slot(0)
+    def relay(near, buf, whole, part, count, peer, first):
+        if count < 8:
+            return {}
+        for k in (2, count - 2):
+            near[k].wait_recv()
+        out = {count // 2: []}
+        for side, k, step in ((0, 2, 1), (1, count - 2, count - 1)):
+            onward = (k + step) % count
+            out[onward] = [remote(whole(buf.at[k]), whole(buf.at[onward]), first + onward, peer(step))]
+        for side, k in ((0, 2), (1, count - 2)):
+            out[count // 2].append(
+                remote(part(buf.at[k], side), part(buf.at[count // 2], side), first + 8 + side, peer(k))
+            )
+        return out
+
+    def key_whole(ref):
+        return ref.at[core]
+
+    def key_part(ref, side):
+        return ref.at[core, :, pl.ds(side * LANES, LANES)]
+
+    def query_whole(ref):
+        return ref
+
+    def query_part(ref, side):
+        return ref.at[pl.ds(side * (qrows // 2), qrows // 2), :]
+
+    qrows = qbuf.shape[1]
+    k_far = relay(k_near, msg, key_whole, key_part, nz, z_peer, 96)
+    q_far = relay(q_near, qbuf, query_whole, query_part, ny, y_peer, 112)
+    arrivals = {k: [k_near[k]] for k in direct(nz)}
+    arrivals.update(k_far)
     forwards = []
-    passed = []
-    for k in near_first(nz):
-        k_copies[k - 1].wait_recv()
-        forward = pltpu.make_async_remote_copy(
-            src_ref=msg.at[k, core],
-            dst_ref=msg.at[k, core],
-            send_sem=fwd_send.at[k],
-            recv_sem=fwd_recv.at[k],
-            device_id=sibling,
-            device_id_type=MESH,
-        )
-        forward.start()
-        forwards.append(forward)
-        passed.append(k)
-        if len(passed) > 1:
+    order = direct(nz) + sorted(k_far, key=lambda k: min(k, nz - k))
+    for k in order:
+        landed(f for f in arrivals[k] if not f.landed)
+        forwards.append(remote(msg.at[k, core], msg.at[k, core], 128 + k, sibling))
+        if len(forwards) > 1:
             forwards[-2].wait_recv()
-            expand_slot(passed[-2])
-    forwards[-1].wait_recv()
-    expand_slot(passed[-1])
+            expand_slot(order[len(forwards) - 2])
+    if forwards:
+        forwards[-1].wait_recv()
+        expand_slot(order[-1])
 
     latent = ctxl[...].astype(BF16)
     rope_k = ctxr[...].T[:ROPE]
@@ -479,28 +503,32 @@
             ostage[j, LANES:, :] = jnp.concatenate([hi, lo, jnp.zeros((12, LANES), F32)], axis=0).astype(BF16)
 
     o_copies = []
-    order = sorted(range(ny), key=lambda j: min(j, ny - j))
+    o_half = []
+    halves = ((0, HD), (HD, ostage.shape[1] - HD))
+    order = sorted(range(ny), key=lambda j: -min(j, ny - j))
+    arrivals = {k: [q_near[k]] for k in direct(ny)}
+    arrivals.update(q_far)
+    arrivals[0] = []
     for at in range(0, ny, 2):
         slots = order[at : at + 2]
         for j in slots:
-            if j:
-                q_copies[j - 1].wait_recv()
+            landed(f for f in arrivals[j] if not f.landed)
         attend(slots)
         for j in slots:
-            if j == 0:
-                continue
-            copy = pltpu.make_async_remote_copy(
-                src_ref=ostage.at[j],
-                dst_ref=obuf.at[j],
-                send_sem=send_sem.at[48 + j],
-                recv_sem=recv_sem.at[48 + j],
-                device_id=y_peer(ny - j),
-                device_id_type=MESH,
-            )
-            copy.start()
-            o_copies.append(copy)
-    for copy in o_copies:
-        copy.wait_recv()
+            if j == 4:
+                for side, step in ((0, 2), (1, ny - 2)):
+                    rows_at = pl.ds(*halves[side])
+                    o_half.append(
+                        remote(ostage.at[j, rows_at, :], opass.at[rows_at, :], 138 + side, y_peer(step))
+                    )
+            elif j:
+                o_copies.append(remote(ostage.at[j], obuf.at[j], 144 + j, y_peer(ny - j)))
+    if o_half:
+        for side, step in ((0, 2), (1, ny - 2)):
+            o_half[side].wait_recv()
+            rows_at = pl.ds(*halves[side])
+            o_copies.append(remote(opass.at[rows_at, :], obuf.at[4, rows_at, :], 152 + side, y_peer(step)))
+    landed(o_copies)
     num = ostage[0, 0:LANES, :].astype(F32)
     den = ostage[0, LANES:, :].astype(F32)
     for j in range(1, ny):
@@ -522,32 +550,19 @@
     proj = jnp.dot(attended, wout[...], preferred_element_type=F32).astype(BF16)
     for t in range(ntp):
         rstage[t] = proj[t * rows : (t + 1) * rows]
-    r_copies = []
-    for k in range(1, ntp):
-        r_copies.append(
-            pltpu.make_async_remote_copy(
-                src_ref=rstage.at[(tp + k) % ntp],
-                dst_ref=rbuf.at[k],
-                send_sem=send_sem.at[56 + k],
-                recv_sem=recv_sem.at[56 + k],
-                device_id=t_peer(k),
-                device_id_type=MESH,
-            )
-        )
-    for copy in r_copies:
-        copy.start()
+    r_copies = [
+        remote(rstage.at[(tp + k) % ntp], rbuf.at[k], 160 + k, t_peer(k)) for k in range(1, ntp)
+    ]
     result = rstage[tp].astype(F32)
-    for copy in r_copies:
-        copy.wait_recv()
+    landed(r_copies)
     for k in range(1, ntp):
         result = result + rbuf[k].astype(F32)
-    for copy in gt_copies:
-        copy.wait_recv()
+    landed(gt_copies)
     gate_row = jnp.concatenate([gtbuf[t] for t in range(ntp)], axis=1)
     out_ref[...] = (gtok[tp].astype(F32) + gate_row * result).astype(BF16)
 
-    for copy in gz_copies + gy_copies + gt_copies + z_copies + tok_copies + y_copies + t_copies + k_copies + q_copies + forwards + o_copies + r_copies:
-        copy.wait_send()
+    for flight in sent:
+        flight.wait_send()
 
 
 def solution(mesh, nz=8):
@@ -620,13 +635,12 @@
                 vm((LANES, LANES), F32),
                 vm((ny, LANES + 16, LANES), BF16),
                 vm((ny, LANES + 16, LANES), BF16),
+                vm((LANES + 16, LANES), BF16),
                 vm((ntp, rows, width), BF16),
                 vm((ntp, rows, width), BF16),
                 pltpu.SemaphoreType.DMA((16,)),
-                pltpu.SemaphoreType.DMA((96,)),
-                pltpu.SemaphoreType.DMA((96,)),
-                pltpu.SemaphoreType.DMA((8,)),
-                pltpu.SemaphoreType.DMA((8,)),
+                pltpu.SemaphoreType.DMA((176,)),
+                pltpu.SemaphoreType.DMA((176,)),
             ],
             compiler_params=pltpu.CompilerParams(
                 collective_id=0, has_side_effects=True, vmem_limit_bytes=60 * 1024 * 1024

time: 63.3 us -> 63.4 us (level)
  no operation moved by 1% of the time
where the time goes in v3:
time: 63.4 us; the launch traced here: 63.2 us
  Pallas kernels  61.7 us (97%)
  local copies, waits for them, and re-layouts  1.47 us (2%)
    pallas_call x1, Pallas kernels, local(): pl.pallas_call(functools.partial(kernel, nz, ny, ntp), out_shape=jax.Shap...  61.7 us
    unnamed x1, local copies, waits for them, and re-layouts  1.47 us

profile of v3, /device:TPU:1, one launch (start us, length us, event | category | flops | bytes accessed | tf_op | source)
XLA Modules:
  0.0 63.2 jit_solution(9924160366814268487)
XLA Ops:
  0.0 61.7 %shard_map.163 = bf16[16,2048]{1,0:T(8,128)(2,1)} custom-call(bf16[16,2048]{1,0:T(8,128)(2,1)} %tok_h.1, bf16[8,2048]{1,0:T(8,128)(2,1)} %ctx_h.1, f32[16,128]{1,0:T(8,128)} %bitcast.11, f32[16,128]{1,0:T(8,128)} %bitcast.12, bf16[32,256]{1,0:T(8,128)(2,1)} %mshift_h.1, bf16[32,256]{1,0:T(8,128)(2,1)} %mscale_h.1, bf16[32,256]{1,0:T(8,128)(2,1)} %mgate_h.1, ...), custom_call_target="tpu_custom_call" | custom-call | tf_op jit(solution)/shard_map/pallas_call | solution.py:598
  61.7 1.5 %copy.19 = bf16[16,2048]{1,0:T(8,128)(2,1)} copy(bf16[16,2048]{1,0:T(8,128)(2,1)} %shard_map.163) | data formatting | bytes 131072

commit v4 on v3

--- a/solution.py
+++ b/solution.py
@@ -136,8 +136,8 @@
     ostage,
     obuf,
     opass,
-    rstage,
-    rbuf,
+    share_out,
+    heads,
     load_sem,
     send_sem,
     recv_sem,
@@ -185,7 +185,7 @@
         (wdown_h, wdown),
         (wrope_h, wrope),
         (wq_h, wq),
-        (wout_h, wout),
+        (wout_h, wout.at[tp]),
     ]
     loads = [pltpu.make_async_copy(a, b, load_sem.at[i]) for i, (a, b) in enumerate(pairs)]
     for copy in loads:
@@ -292,6 +292,19 @@
             )
         tok_side.append(remote(gtok.at[came], gtok.at[came], 24 + k, sibling))
 
+    nx = ntp // 2
+    half_w = width // 2
+
+    def columns(side):
+        return pl.ds(side * half_w, half_w)
+
+    def w_block(index, side):
+        return wout.at[index, :, columns(side)]
+
+    loads[15].wait()
+    w_side = [remote(wout.at[tp], wout.at[tp], 168, sibling)]
+    w_first = {k: remote(w_block(tp, side), w_block(tp, side), 169 + side, x_peer(k)) for side, k in enumerate(near_x)}
+
     landed(z_copies)
     total = zbuf[0]
     for k in range(1, nz):
@@ -333,9 +346,16 @@
 
     lax.fori_loop(0, ntp, norm_rows, 0)
 
-    for i in range(12, 16):
+    for i in range(12, 15):
         loads[i].wait()
     landed(t_copies)
+    w_second = {k: remote(w_block(tp, 1 - side), w_block(tp, 1 - side), 171 + side, x_peer(k)) for side, k in enumerate(near_x)}
+    w_far = []
+    if nx == 4:
+        for side, k in enumerate(near_x):
+            w_first[k].wait_recv()
+            came = x_index(nx - k)
+            w_far.append(remote(w_block(came, side), w_block(came, side), 173 + side, x_peer(k)))
 
     def vector(which, who):
         return jnp.concatenate(
@@ -523,11 +543,24 @@
                     )
             elif j:
                 o_copies.append(remote(ostage.at[j], obuf.at[j], 144 + j, y_peer(ny - j)))
+    def pass_weights():
+        for k in near_x:
+            for flight in (w_first[k], w_second[k]):
+                if not flight.landed:
+                    flight.wait_recv()
+            came = x_index(nx - k)
+            w_side.append(remote(wout.at[came], wout.at[came], 175 + k, sibling))
+        if w_far:
+            landed(w_far)
+            came = x_index(2)
+            w_side.append(remote(wout.at[came], wout.at[came], 179, sibling))
+
     if o_half:
         for side, step in ((0, 2), (1, ny - 2)):
             o_half[side].wait_recv()
             rows_at = pl.ds(*halves[side])
             o_copies.append(remote(opass.at[rows_at, :], obuf.at[4, rows_at, :], 152 + side, y_peer(step)))
+    pass_weights()
     landed(o_copies)
     num = ostage[0, 0:LANES, :].astype(F32)
     den = ostage[0, LANES:, :].astype(F32)
@@ -547,16 +580,15 @@
     spread = jnp.dot(spread, swap, precision=HIGHEST, preferred_element_type=F32)
     attended = (num / spread).astype(BF16)
 
-    proj = jnp.dot(attended, wout[...], preferred_element_type=F32).astype(BF16)
-    for t in range(ntp):
-        rstage[t] = proj[t * rows : (t + 1) * rows]
-    r_copies = [
-        remote(rstage.at[(tp + k) % ntp], rbuf.at[k], 160 + k, t_peer(k)) for k in range(1, ntp)
+    share_out[...] = attended.reshape(ntp, rows, LANES)
+    heads[tp] = share_out[tp]
+    a_copies = [
+        remote(share_out.at[(tp + k) % ntp], heads.at[tp], 160 + k, t_peer(k)) for k in range(1, ntp)
     ]
-    result = rstage[tp].astype(F32)
-    landed(r_copies)
-    for k in range(1, ntp):
-        result = result + rbuf[k].astype(F32)
+    landed(w_side)
+    landed(a_copies)
+    mixed = jnp.concatenate([heads[t] for t in range(ntp)], axis=1)
+    result = jnp.dot(mixed, wout[...].reshape(ntp * LANES, width), preferred_element_type=F32)
     landed(gt_copies)
     gate_row = jnp.concatenate([gtbuf[t] for t in range(ntp)], axis=1)
     out_ref[...] = (gtok[tp].astype(F32) + gate_row * result).astype(BF16)
@@ -614,7 +646,7 @@
                 vm((1, KVL), F32),
                 vm(w_up_kv.shape, BF16),
                 vm((1, QK), F32),
-                vm(w_output.shape, BF16),
+                vm((ntp, *w_output.shape), BF16),
                 vm((nz, 2, 2 * piece), F32),
                 vm((ny, 2, 2 * piece), F32),
                 vm((ntp, 2, 2 * piece), F32),
@@ -636,11 +668,11 @@
                 vm((ny, LANES + 16, LANES), BF16),
                 vm((ny, LANES + 16, LANES), BF16),
                 vm((LANES + 16, LANES), BF16),
-                vm((ntp, rows, width), BF16),
-                vm((ntp, rows, width), BF16),
+                vm((ntp, rows, LANES), BF16),
+                vm((ntp, rows, LANES), BF16),
                 pltpu.SemaphoreType.DMA((16,)),
-                pltpu.SemaphoreType.DMA((176,)),
-                pltpu.SemaphoreType.DMA((176,)),
+                pltpu.SemaphoreType.DMA((184,)),
+                pltpu.SemaphoreType.DMA((184,)),
             ],
             compiler_params=pltpu.CompilerParams(
                 collective_id=0, has_side_effects=True, vmem_limit_bytes=60 * 1024 * 1024

time: 63.4 us -> 60.2 us (0.950)
  Pallas kernels: 61.7 us -> 58.5 us
    pallas_call x1, Pallas kernels: 61.7 us -> 58.5 us  [local(): pl.pallas_call(functools.partial(kernel, nz, ny, ntp), out_shape=jax.Shap...]
where the time goes in v4:
time: 60.2 us; the launch traced here: 60 us
  Pallas kernels  58.5 us (97%)
  local copies, waits for them, and re-layouts  1.47 us (2%)
    pallas_call x1, Pallas kernels, local(): pl.pallas_call(functools.partial(kernel, nz, ny, ntp), out_shape=jax.Shap...  58.5 us
    unnamed x1, local copies, waits for them, and re-layouts  1.47 us

profile of v4, /device:TPU:1, one launch (start us, length us, event | category | flops | bytes accessed | tf_op | source)
XLA Modules:
  0.0 60.0 jit_solution(9948761409424366149)
XLA Ops:
  0.0 58.5 %shard_map.163 = bf16[16,2048]{1,0:T(8,128)(2,1)} custom-call(bf16[16,2048]{1,0:T(8,128)(2,1)} %tok_h.1, bf16[8,2048]{1,0:T(8,128)(2,1)} %ctx_h.1, f32[16,128]{1,0:T(8,128)} %bitcast.11, f32[16,128]{1,0:T(8,128)} %bitcast.12, bf16[32,256]{1,0:T(8,128)(2,1)} %mshift_h.1, bf16[32,256]{1,0:T(8,128)(2,1)} %mscale_h.1, bf16[32,256]{1,0:T(8,128)(2,1)} %mgate_h.1, ...), custom_call_target="tpu_custom_call" | custom-call | tf_op jit(solution)/shard_map/pallas_call | solution.py:630
  58.5 1.5 %copy.19 = bf16[16,2048]{1,0:T(8,128)(2,1)} copy(bf16[16,2048]{1,0:T(8,128)(2,1)} %shard_map.163) | data formatting | bytes 131072

commit v5 on v4

--- a/solution.py
+++ b/solution.py
@@ -136,6 +136,8 @@
     ostage,
     obuf,
     opass,
+    osum,
+    onext,
     share_out,
     heads,
     load_sem,
@@ -522,27 +524,67 @@
             ostage[j, 0:LANES, :] = jnp.where(low, first, second).astype(BF16)
             ostage[j, LANES:, :] = jnp.concatenate([hi, lo, jnp.zeros((12, LANES), F32)], axis=0).astype(BF16)
 
+    def packed_rows(ref):
+        block = ref[...].astype(F32)
+        return block[:LANES], block[LANES : LANES + 2] + block[LANES + 2 : LANES + 4]
+
+    def store_packed(ref, num, den):
+        hi = den.astype(BF16).astype(F32)
+        ref[0:LANES, :] = num.astype(BF16)
+        ref[LANES:, :] = jnp.concatenate([hi, den - hi, jnp.zeros((12, LANES), F32)], axis=0).astype(BF16)
+
     o_copies = []
-    o_half = []
+    o_add = {}
     halves = ((0, HD), (HD, ostage.shape[1] - HD))
-    order = sorted(range(ny), key=lambda j: -min(j, ny - j))
     arrivals = {k: [q_near[k]] for k in direct(ny)}
     arrivals.update(q_far)
     arrivals[0] = []
+    joined = ny >= 8
+    if joined:
+        order = [3, ny - 3, ny // 2, 0, 2, ny - 2, 1, ny - 1]
+    else:
+        order = sorted(range(ny), key=lambda j: -min(j, ny - j))
     for at in range(0, ny, 2):
         slots = order[at : at + 2]
         for j in slots:
             landed(f for f in arrivals[j] if not f.landed)
         attend(slots)
         for j in slots:
-            if j == 4:
-                for side, step in ((0, 2), (1, ny - 2)):
+            if j == 0 or (joined and j in (2, ny - 2)):
+                continue
+            if joined and j in (3, ny - 3):
+                side = 0 if j == 3 else 1
+                o_add[side] = [remote(ostage.at[j], osum.at[side], 138 + side, y_peer(ny - 1 if side == 0 else 1))]
+            elif joined and j == ny // 2:
+                for side in range(2):
                     rows_at = pl.ds(*halves[side])
-                    o_half.append(
-                        remote(ostage.at[j, rows_at, :], opass.at[rows_at, :], 138 + side, y_peer(step))
+                    o_add[side].append(
+                        remote(
+                            ostage.at[j, rows_at, :],
+                            opass.at[rows_at, :],
+                            140 + side,
+                            y_peer(ny - 2 if side == 0 else 2),
+                        )
                     )
-            elif j:
+            else:
                 o_copies.append(remote(ostage.at[j], obuf.at[j], 144 + j, y_peer(ny - j)))
+    if joined:
+        for side in range(2):
+            landed(o_add[side])
+        passed_num, passed_den = packed_rows(opass)
+        for side, j in ((0, 2), (1, ny - 2)):
+            num, den = packed_rows(ostage.at[j])
+            more_num, more_den = packed_rows(osum.at[side])
+            blank = jnp.zeros((HD, LANES), F32)
+            if side == 0:
+                extra = jnp.concatenate([passed_num[:HD], blank], axis=0)
+            else:
+                extra = jnp.concatenate([blank, passed_num[HD:]], axis=0)
+                more_den = more_den + passed_den
+            store_packed(onext.at[side], num + more_num + extra, den + more_den)
+            o_copies.append(remote(onext.at[side], obuf.at[j], 144 + j, y_peer(ny - j)))
+    sources = [k for k in range(1, ny) if not joined or k in (1, 2, ny - 2, ny - 1)]
+
     def pass_weights():
         for k in near_x:
             for flight in (w_first[k], w_second[k]):
@@ -555,16 +597,11 @@
             came = x_index(2)
             w_side.append(remote(wout.at[came], wout.at[came], 179, sibling))
 
-    if o_half:
-        for side, step in ((0, 2), (1, ny - 2)):
-            o_half[side].wait_recv()
-            rows_at = pl.ds(*halves[side])
-            o_copies.append(remote(opass.at[rows_at, :], obuf.at[4, rows_at, :], 152 + side, y_peer(step)))
     pass_weights()
     landed(o_copies)
     num = ostage[0, 0:LANES, :].astype(F32)
     den = ostage[0, LANES:, :].astype(F32)
-    for j in range(1, ny):
+    for j in sources:
         num = num + obuf[j, 0:LANES, :].astype(F32)
         den = den + obuf[j, LANES:, :].astype(F32)
     den = den[0:2] + den[2:4]
@@ -591,7 +628,7 @@
     result = jnp.dot(mixed, wout[...].reshape(ntp * LANES, width), preferred_element_type=F32)
     landed(gt_copies)
     gate_row = jnp.concatenate([gtbuf[t] for t in range(ntp)], axis=1)
-    out_ref[...] = (gtok[tp].astype(F32) + gate_row * result).astype(BF16)
+    out_ref[...] = gate_row * result
 
     for flight in sent:
         flight.wait_send()
@@ -627,9 +664,9 @@
         vm = pltpu.VMEM
         anywhere = pl.BlockSpec(memory_space=pl.ANY)
         smem = pl.BlockSpec(memory_space=pltpu.SMEM)
-        return pl.pallas_call(
+        update = pl.pallas_call(
             functools.partial(kernel, nz, ny, ntp),
-            out_shape=jax.ShapeDtypeStruct((rows, width), BF16),
+            out_shape=jax.ShapeDtypeStruct((rows, width), F32),
             in_specs=[anywhere] * 15 + [smem, anywhere],
             out_specs=pl.BlockSpec(memory_space=pltpu.VMEM),
             scratch_shapes=[
@@ -668,6 +705,8 @@
                 vm((ny, LANES + 16, LANES), BF16),
                 vm((ny, LANES + 16, LANES), BF16),
                 vm((LANES + 16, LANES), BF16),
+                vm((2, LANES + 16, LANES), BF16),
+                vm((2, LANES + 16, LANES), BF16),
                 vm((ntp, rows, LANES), BF16),
                 vm((ntp, rows, LANES), BF16),
                 pltpu.SemaphoreType.DMA((16,)),
@@ -696,6 +735,7 @@
             ctx_lift.reshape(1, 2),
             w_output,
         )
+        return (latent_tokens.astype(F32) + update).astype(BF16)
 
     in_specs = (
         P(("sp", "tp"), None),

time: 60.2 us -> 60.7 us (level)
  other arithmetic: 0 us -> 1.55 us
  local copies, waits for them, and re-layouts: 1.47 us -> 0.01 us
    convert_element_type x0 -> x1, other arithmetic: none -> 1.55 us  [local(): return (latent_tokens.astype(F32) + update).astype(BF16)]
    unnamed x1 -> x2, local copies, waits for them, and re-layouts: 1.47 us -> 0.01 us
where the time goes in v5:
time: 60.7 us; the launch traced here: 60.5 us
  Pallas kernels  59 us (97%)
  other arithmetic  1.55 us (3%)
    pallas_call x1, Pallas kernels, local(): pl.pallas_call(functools.partial(kernel, nz, ny, ntp), out_shape=jax.Shap...  59 us
    convert_element_type x1, other arithmetic, local(): return (latent_tokens.astype(F32) + update).astype(BF16)  1.55 us

profile of v5, /device:TPU:1, one launch (start us, length us, event | category | flops | bytes accessed | tf_op | source)
XLA Modules:
  0.0 60.5 jit_solution(15439812383025418226)
XLA Ops:
  0.0 0.0 copy-start
  0.0 59.0 %shard_map.163 = f32[16,2048]{1,0:T(8,128)} custom-call(bf16[16,2048]{1,0:T(8,128)(2,1)} %tok_h.1, bf16[8,2048]{1,0:T(8,128)(2,1)} %ctx_h.1, f32[16,128]{1,0:T(8,128)} %bitcast.11, f32[16,128]{1,0:T(8,128)} %bitcast.12, bf16[32,256]{1,0:T(8,128)(2,1)} %mshift_h.1, bf16[32,256]{1,0:T(8,128)(2,1)} %mscale_h.1, bf16[32,256]{1,0:T(8,128)(2,1)} %mgate_h.1, ...), custom_call_target="tpu_custom_call" | custom-call | tf_op jit(solution)/shard_map/pallas_call | solution.py:667
  59.0 0.0 copy-done
  59.0 1.5 %add_convert_fusion = bf16[16,2048]{1,0:T(8,128)(2,1)} fusion(f32[16,2048]{1,0:T(8,128)} %shard_map.163, bf16[16,2048]{1,0:T(8,128)(2,1)S(1)} %copy-done), kind=kLoop, calls=%fused_computation | loop fusion | flops 98304 | bytes 262144 | tf_op jit(solution)/shard_map/convert_element_type | solution.py:738
Async XLA Ops:
  0.0 59.0 %copy-start = (bf16[16,2048]{1,0:T(8,128)(2,1)S(1)}, bf16[16,2048]{1,0:T(8,128)(2,1)}, u32[]{:S(2)}) copy-start(bf16[16,2048]{1,0:T(8,128)(2,1)} %tok_h.1) | copy-start | bytes 196612

commit v6 on v4

--- a/solution.py
+++ b/solution.py
@@ -131,6 +131,7 @@
     qbuf,
     keys,
     vals,
+    near_sum,
     ctxl,
     ctxr,
     ostage,
@@ -408,12 +409,15 @@
     qbuf[0, LANES:, :] = tail[: LANES // 2].astype(BF16)
     q_near = {k: remote(qbuf.at[0], qbuf.at[k], 80 + k, y_peer(k)) for k in direct(ny)}
 
+    place = {k: at for at, k in enumerate([0] + direct(nz) + [k for k in range(1, nz) if k not in direct(nz)])}
+    near_keys = (1 + len(direct(nz))) * LANES
+
     def expand_slot(k):
         latent = msg[k, :, 0:64, :].reshape(LANES, KVL)
         rope_k = jnp.concatenate([msg[k, 0, 64:80, 0:LANES], msg[k, 1, 64:80, 0:LANES]], axis=0).astype(F32)
         up = nt_dot(wupt[...], latent)
         shared = jnp.sum(rope_k * rope_k, axis=0, keepdims=True)
-        at = pl.ds(k * LANES, LANES)
+        at = pl.ds(place[k] * LANES, LANES)
         for h in range(2):
             part = up[h * HD : (h + 1) * HD]
             inv = lax.rsqrt((jnp.sum(part * part, axis=0, keepdims=True) + shared) * (1.0 / QK) + EPS)
@@ -427,6 +431,49 @@
         ctx_two = msg[k, 0, 64:80, LANES:].astype(F32)
         ctxl[k * crow : (k + 1) * crow, :] = jnp.concatenate([ctx_two[:crow], ctx_two[8 : 8 + crow]], axis=1)
         ctxr[k * crow : (k + 1) * crow, :] = msg[k, 1, 64:80, LANES:].astype(F32)[:crow]
+
+    diagonal = lane_ids((LANES, LANES)) % HD == row_ids((LANES, LANES)) % HD
+    low = lane_ids((LANES, LANES)) < HD
+    late = lane_ids((1, nlat + LANES)) < nlat
+    lifts = [jnp.where(late, lift_s[0, h] * LOG2E, 0.0) for h in range(2)]
+
+    def whole_query(j):
+        tails = qbuf[j, LANES:, :]
+        turned_tails = pltpu.roll(tails.astype(F32), LANES // 2, 1).astype(BF16)
+        return jnp.concatenate([qbuf[j, 0:LANES, :], jnp.concatenate([tails, turned_tails], axis=0)], axis=1)
+
+    def mix(slots, start, stop):
+        q = jnp.concatenate([whole_query(j) for j in slots], axis=0)
+        outs = []
+        for h in range(2):
+            s = jnp.dot(q, keys[h, :, start:stop], preferred_element_type=F32)
+            p = jnp.exp2(s - lifts[h][:, start:stop]).astype(BF16)
+            outs.append(jnp.dot(p, vals[h, start:stop, :], preferred_element_type=F32))
+        return outs
+
+    def mix_near(slots):
+        for h, out in enumerate(mix(slots, 0, near_keys)):
+            for i, j in enumerate(slots):
+                near_sum[h, j] = out[i * LANES : (i + 1) * LANES]
+
+    def attend(slots, begun):
+        outs = mix(slots, near_keys if begun else 0, nlat + LANES)
+        for i, j in enumerate(slots):
+            first, second = (out[i * LANES : (i + 1) * LANES] for out in outs)
+            if begun:
+                first, second = first + near_sum[0, j], second + near_sum[1, j]
+            den = jnp.where(diagonal, jnp.where(low, second, first), 0.0)
+            packed = jnp.concatenate(
+                [
+                    jnp.sum(den[:HD], axis=0, keepdims=True),
+                    jnp.sum(den[HD:], axis=0, keepdims=True),
+                ],
+                axis=0,
+            )
+            hi = packed.astype(BF16).astype(F32)
+            lo = packed - hi
+            ostage[j, 0:LANES, :] = jnp.where(low, first, second).astype(BF16)
+            ostage[j, LANES:, :] = jnp.concatenate([hi, lo, jnp.zeros((12, LANES), F32)], axis=0).astype(BF16)
 
     expand_slot(0)
     def relay(near, buf, whole, part, count, peer, first):
@@ -447,7 +494,7 @@
     def key_whole(ref):
         return ref.at[core]
 
-    def key_part(ref, side):
+    def key_piece(ref, side):
         return ref.at[core, :, pl.ds(side * LANES, LANES)]
 
     def query_whole(ref):
@@ -457,21 +504,28 @@
         return ref.at[pl.ds(side * (qrows // 2), qrows // 2), :]
 
     qrows = qbuf.shape[1]
-    k_far = relay(k_near, msg, key_whole, key_part, nz, z_peer, 96)
+    k_far = relay(k_near, msg, key_whole, key_piece, nz, z_peer, 96)
     q_far = relay(q_near, qbuf, query_whole, query_part, ny, y_peer, 112)
     arrivals = {k: [k_near[k]] for k in direct(nz)}
     arrivals.update(k_far)
-    forwards = []
-    order = direct(nz) + sorted(k_far, key=lambda k: min(k, nz - k))
-    for k in order:
-        landed(f for f in arrivals[k] if not f.landed)
-        forwards.append(remote(msg.at[k, core], msg.at[k, core], 128 + k, sibling))
-        if len(forwards) > 1:
-            forwards[-2].wait_recv()
-            expand_slot(order[len(forwards) - 2])
-    if forwards:
-        forwards[-1].wait_recv()
-        expand_slot(order[-1])
+    def take_keys(order):
+        forwards = []
+        for at, k in enumerate(order):
+            landed(f for f in arrivals[k] if not f.landed)
+            forwards.append(remote(msg.at[k, core], msg.at[k, core], 128 + k, sibling))
+            if at > 0:
+                forwards[at - 1].wait_recv()
+                expand_slot(order[at - 1])
+        if order:
+            forwards[-1].wait_recv()
+            expand_slot(order[-1])
+
+    take_keys(direct(nz))
+    near_slots = direct(ny) + [0]
+    landed(q_near[k] for k in direct(ny) if not q_near[k].landed)
+    for at in range(0, len(near_slots), 3):
+        mix_near(near_slots[at : at + 3])
+    take_keys(sorted(k_far, key=lambda k: min(k, nz - k)))
 
     latent = ctxl[...].astype(BF16)
     rope_k = ctxr[...].T[:ROPE]
@@ -490,52 +544,19 @@
     vals[0, at, :] = jnp.where(low, value, ones).astype(BF16)
     vals[1, at, :] = jnp.where(low, ones, value).astype(BF16)
 
-    diagonal = lane_ids((LANES, LANES)) % HD == row_ids((LANES, LANES)) % HD
-
-    low = lane_ids((LANES, LANES)) < HD
-    late = lane_ids((1, nlat + LANES)) < nlat
-    lifts = [jnp.where(late, lift_s[0, h] * LOG2E, 0.0) for h in range(2)]
-
-    def whole_query(j):
-        tails = qbuf[j, LANES:, :]
-        turned_tails = pltpu.roll(tails.astype(F32), LANES // 2, 1).astype(BF16)
-        return jnp.concatenate([qbuf[j, 0:LANES, :], jnp.concatenate([tails, turned_tails], axis=0)], axis=1)
-
-    def attend(slots):
-        q = jnp.concatenate([whole_query(j) for j in slots], axis=0)
-        outs = []
-        for h in range(2):
-            p = jnp.exp2(jnp.dot(q, keys[h], preferred_element_type=F32) - lifts[h]).astype(BF16)
-            outs.append(jnp.dot(p, vals[h], preferred_element_type=F32))
-        for i, j in enumerate(slots):
-            first, second = (out[i * LANES : (i + 1) * LANES] for out in outs)
-            den = jnp.where(diagonal, jnp.where(low, second, first), 0.0)
-            packed = jnp.concatenate(
-                [
-                    jnp.sum(den[:HD], axis=0, keepdims=True),
-                    jnp.sum(den[HD:], axis=0, keepdims=True),
-                ],
-                axis=0,
-            )
-            hi = packed.astype(BF16).astype(F32)
-            lo = packed - hi
-            ostage[j, 0:LANES, :] = jnp.where(low, first, second).astype(BF16)
-            ostage[j, LANES:, :] = jnp.concatenate([hi, lo, jnp.zeros((12, LANES), F32)], axis=0).astype(BF16)
-
     o_copies = []
     o_half = []
     halves = ((0, HD), (HD, ostage.shape[1] - HD))
-    order = sorted(range(ny), key=lambda j: -min(j, ny - j))
-    arrivals = {k: [q_near[k]] for k in direct(ny)}
-    arrivals.update(q_far)
-    arrivals[0] = []
-    for at in range(0, ny, 2):
-        slots = order[at : at + 2]
+    groups = [(list(q_far), False)] if q_far else []
+    tail_slots = near_slots[:-1]
+    groups += [(tail_slots[at : at + 2], True) for at in range(0, len(tail_slots), 2)] or [([], True)]
+    groups[-1][0].append(0)
+    for slots, begun in groups:
+        if not begun:
+            landed(f for j in slots for f in q_far[j] if not f.landed)
+        attend(slots, begun)
         for j in slots:
-            landed(f for f in arrivals[j] if not f.landed)
-        attend(slots)
-        for j in slots:
-            if j == 4:
+            if j == 4 and ny == 8:
                 for side, step in ((0, 2), (1, ny - 2)):
                     rows_at = pl.ds(*halves[side])
                     o_half.append(
@@ -663,6 +684,7 @@
                 vm((ny, LANES + HD, LANES), BF16),
                 vm((2, 2 * LANES, lat + LANES), BF16),
                 vm((2, lat + LANES, LANES), BF16),
+                vm((2, ny, LANES, LANES), F32),
                 vm((LANES, KVL), F32),
                 vm((LANES, LANES), F32),
                 vm((ny, LANES + 16, LANES), BF16),

time: 60.2 us -> 61.3 us (1.018)
  Pallas kernels: 58.5 us -> 59.6 us
    pallas_call x1, Pallas kernels: 58.5 us -> 59.6 us  [local(): pl.pallas_call(functools.partial(kernel, nz, ny, ntp), out_shape=jax.Shap...]
where the time goes in v6:
time: 61.3 us; the launch traced here: 61.1 us
  Pallas kernels  59.6 us (97%)
  local copies, waits for them, and re-layouts  1.47 us (2%)
    pallas_call x1, Pallas kernels, local(): pl.pallas_call(functools.partial(kernel, nz, ny, ntp), out_shape=jax.Shap...  59.6 us
    unnamed x1, local copies, waits for them, and re-layouts  1.47 us

profile of v6, /device:TPU:1, one launch (start us, length us, event | category | flops | bytes accessed | tf_op | source)
XLA Modules:
  0.0 61.1 jit_solution(16670214276858421148)
XLA Ops:
  0.0 59.6 %shard_map.163 = bf16[16,2048]{1,0:T(8,128)(2,1)} custom-call(bf16[16,2048]{1,0:T(8,128)(2,1)} %tok_h.1, bf16[8,2048]{1,0:T(8,128)(2,1)} %ctx_h.1, f32[16,128]{1,0:T(8,128)} %bitcast.11, f32[16,128]{1,0:T(8,128)} %bitcast.12, bf16[32,256]{1,0:T(8,128)(2,1)} %mshift_h.1, bf16[32,256]{1,0:T(8,128)(2,1)} %mscale_h.1, bf16[32,256]{1,0:T(8,128)(2,1)} %mgate_h.1, ...), custom_call_target="tpu_custom_call" | custom-call | tf_op jit(solution)/shard_map/pallas_call | solution.py:651
  59.6 1.5 %copy.19 = bf16[16,2048]{1,0:T(8,128)(2,1)} copy(bf16[16,2048]{1,0:T(8,128)(2,1)} %shard_map.163) | data formatting | bytes 131072

commit v7 on v4

--- a/solution.py
+++ b/solution.py
@@ -135,7 +135,8 @@
     ctxr,
     ostage,
     obuf,
-    opass,
+    dstage,
+    dbuf,
     share_out,
     heads,
     load_sem,
@@ -517,14 +518,10 @@
                 ],
                 axis=0,
             )
-            hi = packed.astype(BF16).astype(F32)
-            lo = packed - hi
             ostage[j, 0:LANES, :] = jnp.where(low, first, second).astype(BF16)
-            ostage[j, LANES:, :] = jnp.concatenate([hi, lo, jnp.zeros((12, LANES), F32)], axis=0).astype(BF16)
+            dstage[j] = packed
 
     o_copies = []
-    o_half = []
-    halves = ((0, HD), (HD, ostage.shape[1] - HD))
     order = sorted(range(ny), key=lambda j: -min(j, ny - j))
     arrivals = {k: [q_near[k]] for k in direct(ny)}
     arrivals.update(q_far)
@@ -535,13 +532,9 @@
             landed(f for f in arrivals[j] if not f.landed)
         attend(slots)
         for j in slots:
-            if j == 4:
-                for side, step in ((0, 2), (1, ny - 2)):
-                    rows_at = pl.ds(*halves[side])
-                    o_half.append(
-                        remote(ostage.at[j, rows_at, :], opass.at[rows_at, :], 138 + side, y_peer(step))
-                    )
-            elif j:
+            if j:
+                o_copies.append(remote(dstage.at[j], dbuf.at[j], 184 + j, y_peer(ny - j)))
+            if j:
                 o_copies.append(remote(ostage.at[j], obuf.at[j], 144 + j, y_peer(ny - j)))
     def pass_weights():
         for k in near_x:
@@ -555,19 +548,13 @@
             came = x_index(2)
             w_side.append(remote(wout.at[came], wout.at[came], 179, sibling))
 
-    if o_half:
-        for side, step in ((0, 2), (1, ny - 2)):
-            o_half[side].wait_recv()
-            rows_at = pl.ds(*halves[side])
-            o_copies.append(remote(opass.at[rows_at, :], obuf.at[4, rows_at, :], 152 + side, y_peer(step)))
     pass_weights()
     landed(o_copies)
     num = ostage[0, 0:LANES, :].astype(F32)
-    den = ostage[0, LANES:, :].astype(F32)
+    den = dstage[0]
     for j in range(1, ny):
         num = num + obuf[j, 0:LANES, :].astype(F32)
-        den = den + obuf[j, LANES:, :].astype(F32)
-    den = den[0:2] + den[2:4]
+        den = den + dbuf[j]
     spread = jnp.concatenate(
         [
             jnp.broadcast_to(den[0:1], (HD, LANES)),
@@ -665,14 +652,15 @@
                 vm((2, lat + LANES, LANES), BF16),
                 vm((LANES, KVL), F32),
                 vm((LANES, LANES), F32),
-                vm((ny, LANES + 16, LANES), BF16),
-                vm((ny, LANES + 16, LANES), BF16),
-                vm((LANES + 16, LANES), BF16),
+                vm((ny, LANES, LANES), BF16),
+                vm((ny, LANES, LANES), BF16),
+                vm((ny, 2, LANES), F32),
+                vm((ny, 2, LANES), F32),
                 vm((ntp, rows, LANES), BF16),
                 vm((ntp, rows, LANES), BF16),
                 pltpu.SemaphoreType.DMA((16,)),
-                pltpu.SemaphoreType.DMA((184,)),
-                pltpu.SemaphoreType.DMA((184,)),
+                pltpu.SemaphoreType.DMA((192,)),
+                pltpu.SemaphoreType.DMA((192,)),
             ],
             compiler_params=pltpu.CompilerParams(
                 collective_id=0, has_side_effects=True, vmem_limit_bytes=60 * 1024 * 1024

time: 60.2 us -> 59.6 us (0.990)
  no operation moved by 1% of the time
where the time goes in v7:
time: 59.6 us; the launch traced here: 59.4 us
  Pallas kernels  57.9 us (97%)
  local copies, waits for them, and re-layouts  1.47 us (2%)
    pallas_call x1, Pallas kernels, local(): pl.pallas_call(functools.partial(kernel, nz, ny, ntp), out_shape=jax.Shap...  57.9 us
    unnamed x1, local copies, waits for them, and re-layouts  1.47 us

profile of v7, /device:TPU:1, one launch (start us, length us, event | category | flops | bytes accessed | tf_op | source)
XLA Modules:
  0.0 59.4 jit_solution(6937935467753334606)
XLA Ops:
  0.0 57.9 %shard_map.163 = bf16[16,2048]{1,0:T(8,128)(2,1)} custom-call(bf16[16,2048]{1,0:T(8,128)(2,1)} %tok_h.1, bf16[8,2048]{1,0:T(8,128)(2,1)} %ctx_h.1, f32[16,128]{1,0:T(8,128)} %bitcast.11, f32[16,128]{1,0:T(8,128)} %bitcast.12, bf16[32,256]{1,0:T(8,128)(2,1)} %mshift_h.1, bf16[32,256]{1,0:T(8,128)(2,1)} %mscale_h.1, bf16[32,256]{1,0:T(8,128)(2,1)} %mgate_h.1, ...), custom_call_target="tpu_custom_call" | custom-call | tf_op jit(solution)/shard_map/pallas_call | solution.py:617
  58.0 1.5 %copy.19 = bf16[16,2048]{1,0:T(8,128)(2,1)} copy(bf16[16,2048]{1,0:T(8,128)(2,1)} %shard_map.163) | data formatting | bytes 131072
